TPU v7x, 512 devices: a whole 4x4x16 slice. The times are simulated.
512 devices in a mesh: ep: 32 (over z, core), tp: 16 (over y, x).
Axes of the slice: x: 4, y: 4, z: 16, core: 2. Of those that a mesh axis runs over, the one named last changes fastest.
Arguments:
- mix_input: bfloat16 [4096, 2048], P('ep'), may hold values from -8 to 8
- expert_input: bfloat16 [4096, 2048], P('ep'), may hold values from -8 to 8
- mix_gain: float32 [2048], replicated, may hold values from 0.1 to 1.9
- moe_gain: float32 [2048], replicated, may hold values from 0.1 to 1.9
- pool_in: bfloat16 [2048, 1024], P(None, 'tp'), may hold values from -0.125 to 0.125
- pool_scale: float32 [1024], P('tp'), may hold values from 0.25 to 10
- pool_gain: float32 [1024], P('tp'), may hold values from 0.1 to 1.9
- pool_out: bfloat16 [1024, 2048], P(None, 'tp'), may hold values from -0.1875 to 0.1875
- route: int32 [4096, 4], P('ep'), may hold values from 0 to 31, all different within a row; in each aligned block of 128 rows (0 to 127, 128 to 255, ...) at most 32 rows name the same one
- route_score: float32 [4096, 4], P('ep'), may hold values from 0.05 to 1
- expert_gate: bfloat16 [32, 2048, 2048], P('ep', None, 'tp'), may hold values from -0.125 to 0.125
- expert_up: bfloat16 [32, 2048, 2048], P('ep', None, 'tp'), may hold values from -0.125 to 0.125
- expert_down: bfloat16 [32, 2048, 2048], P('ep', 'tp'), may hold values from -0.1875 to 0.1875
- shared_gate: bfloat16 [2048, 2048], P(None, 'tp'), may hold values from -0.125 to 0.125
- shared_up: bfloat16 [2048, 2048], P(None, 'tp'), may hold values from -0.125 to 0.125
- shared_down: bfloat16 [2048, 2048], P(None, 'tp'), may hold values from -0.125 to 0.125
Outputs:
- mix_out: bfloat16 [4096, 2048], P('ep', 'tp')
- moe_out: bfloat16 [4096, 2048], P('ep', 'tp')
Inputs may be any that keep to these rules, and one draw needn't show every extreme that they name: `route`: each row names 4 different experts. In the rows of one index of ep (aligned blocks of 128 rows) no expert is named more than 32 times, a bound that some block reaches.
All inputs are finite; a program needn't handle non-finite values.
Results may differ from a plain program's by a relative error of at most 0.014.
Values may be sent and summed in bfloat16 or wider, within the bound.
A program may use at most 64 MiB of HBM per device.

v0:
```python
import jax
import jax.numpy as jnp
from jax import lax
from jax.sharding import PartitionSpec as P

epsilon = 1e-06
reach_rows = 15
window_widths = (2, 4, 8, 16)


def cut_along(array, dim, devices):
    dims = array.shape
    tiles = array.reshape(*dims[:dim], devices, dims[dim] // devices, *dims[dim + 1 :])
    return jnp.moveaxis(tiles, dim, 0)


def sum_at_owner(array, axis, dim):
    tiles = cut_along(array, dim, lax.axis_size(axis))
    arrived = lax.all_to_all(tiles, axis, split_axis=0, concat_axis=0, tiled=True)
    return arrived.astype(jnp.float32).sum(axis=0)


def shifted(block, axis, distance):
    devices = range(lax.axis_size(axis))
    route = [(i - distance, i) for i in devices if i - distance in devices]
    return lax.ppermute(block, axis, route)


def copy_for_each(array, axis):
    copies = jnp.broadcast_to(array, (lax.axis_size(axis), *array.shape))
    return lax.all_to_all(copies, axis, split_axis=0, concat_axis=0, tiled=True)


def of_everyone(array, axis):
    return copy_for_each(array, axis).sum(axis=0)


def in_order(tiles, dim):
    tiles = jnp.moveaxis(tiles, 0, dim)
    dims = tiles.shape
    return tiles.reshape(*dims[:dim], dims[dim] * dims[dim + 1], *dims[dim + 2 :])


def gather_together(arrays, axis, dims):
    ravelled = jnp.concatenate([a.reshape(-1) for a in arrays])
    lines, at, done = (lax.all_gather(ravelled, axis), 0, [])
    for a, dim in zip(arrays, dims):
        tiles = lines[:, at : at + a.size].reshape(-1, *a.shape)
        done.append(in_order(tiles, dim))
        at += a.size
    return tuple(done)


def row_norm(rows, gain):
    values = rows.astype(jnp.float32)
    scale = lax.rsqrt(jnp.mean(values * values, axis=-1, keepdims=True) + epsilon)
    return (values * scale * gain).astype(jnp.bfloat16)


def window_means(extended, position, group, n_rows):
    total = jnp.zeros((n_rows, extended.shape[1]), jnp.float32)
    result = jnp.zeros((n_rows, extended.shape[1]), jnp.float32)
    for lag in range(16):
        total = total + extended[reach_rows - lag : reach_rows - lag + n_rows]
        for index, width in enumerate(window_widths):
            if lag + 1 == width:
                count = jnp.minimum(position, float(width))[:, None]
                result = jnp.where(group[None, :] == index, total / count, result)
    return result - extended[reach_rows:]


def serve(sending, expert_gate, expert_up, expert_down):
    feature_share = sending.shape[3] // lax.axis_size("tp")
    own_part = lax.dynamic_slice_in_dim(
        sending, lax.axis_index("tp") * feature_share, feature_share, 3
    )
    moved = lax.all_to_all(own_part, "ep", split_axis=0, concat_axis=0, tiled=True)
    arrived = lax.all_gather(moved, "tp", axis=3, tiled=True)
    gate = jnp.einsum("send,edf->senf", arrived, expert_gate, preferred_element_type=jnp.float32)
    upper = jnp.einsum("send,edf->senf", arrived, expert_up, preferred_element_type=jnp.float32)
    hidden = (jax.nn.silu(gate) * upper).astype(jnp.bfloat16)
    term = jnp.einsum("senf,efd->send", hidden, expert_down, preferred_element_type=jnp.float32)
    summed = sum_at_owner(term.astype(jnp.bfloat16), "tp", 3).astype(jnp.bfloat16)
    return lax.all_to_all(summed, "ep", split_axis=0, concat_axis=0, tiled=True)


def on_device(
    mix_input,
    expert_input,
    mix_gain,
    moe_gain,
    pool_in,
    pool_scale,
    pool_gain,
    pool_out,
    route,
    route_score,
    expert_gate,
    expert_up,
    expert_down,
    shared_gate,
    shared_up,
    shared_down,
):
    tok_rows = mix_input.shape[0]
    channels = pool_in.shape[1]
    pool_width = channels * lax.axis_size("tp")
    mix_norm = row_norm(mix_input, mix_gain)
    pool_input = jnp.dot(mix_norm, pool_in, preferred_element_type=jnp.float32).astype(jnp.bfloat16)
    before = shifted(pool_input[tok_rows - reach_rows :], "ep", 1)
    extended = jnp.concatenate([before, pool_input], axis=0).astype(jnp.float32)
    position = (lax.axis_index("ep") * tok_rows + jnp.arange(tok_rows, dtype=jnp.int32) + 1).astype(
        jnp.float32
    )
    channel_ids = lax.axis_index("tp") * channels + jnp.arange(channels, dtype=jnp.int32)
    group = channel_ids // (pool_width // 4)
    scaled = window_means(extended, position, group, tok_rows) * pool_scale
    squares = of_everyone(jnp.sum(scaled * scaled, axis=1), "tp")
    pooled_norm = (scaled * lax.rsqrt(squares / pool_width + epsilon)[:, None] * pool_gain).astype(
        jnp.bfloat16
    )
    moe_norm = row_norm(expert_input, moe_gain)
    shared_hidden = (
        jax.nn.silu(jnp.dot(moe_norm, shared_gate, preferred_element_type=jnp.float32))
        * jnp.dot(moe_norm, shared_up, preferred_element_type=jnp.float32)
    ).astype(jnp.bfloat16)
    pooled_all, shared_all = gather_together((pooled_norm, shared_hidden), "tp", (1, 1))
    mix_out = jnp.dot(pooled_all, pool_out, preferred_element_type=jnp.float32).astype(jnp.bfloat16)
    shared_part = jnp.dot(shared_all, shared_down, preferred_element_type=jnp.float32)
    n_tok, top = route.shape
    local_experts = expert_gate.shape[0]
    experts = local_experts * lax.axis_size("ep")
    capacity = 2 * n_tok * top // experts
    flat_route = route.reshape(-1)
    table = (flat_route[:, None] == jnp.arange(experts, dtype=jnp.int32)[None, :]).astype(jnp.int32)
    ranks = jnp.sum((jnp.cumsum(table, axis=0) - table) * table, axis=1)
    slot = flat_route * capacity + ranks
    owner = (
        jnp.full((experts * capacity,), n_tok, jnp.int32)
        .at[slot]
        .set(jnp.arange(n_tok * top, dtype=jnp.int32) // top)
    )
    padded_rows = jnp.concatenate(
        [moe_norm, jnp.zeros((1, moe_norm.shape[1]), jnp.bfloat16)], axis=0
    )
    outgoing = padded_rows[owner].reshape(
        lax.axis_size("ep"), local_experts, capacity, moe_norm.shape[1]
    )
    returned = serve(outgoing, expert_gate, expert_up, expert_down)
    back_rows = returned.reshape(experts * capacity, returned.shape[3])
    picked = back_rows[slot].reshape(n_tok, top, returned.shape[3]).astype(jnp.float32)
    weights = 2.5 * route_score / jnp.sum(route_score, axis=1, keepdims=True)
    routed = jnp.sum(picked * weights[:, :, None], axis=1)
    moe_out = (routed + shared_part).astype(jnp.bfloat16)
    return (mix_out, moe_out)


def solution(mesh):
    return jax.shard_map(
        on_device,
        mesh=mesh,
        in_specs=(
            P("ep", None),
            P("ep", None),
            P(),
            P(),
            P(None, "tp"),
            P("tp"),
            P("tp"),
            P(None, "tp"),
            P("ep", None),
            P("ep", None),
            P("ep", None, "tp"),
            P("ep", None, "tp"),
            P("ep", "tp", None),
            P(None, "tp"),
            P(None, "tp"),
            P(None, "tp"),
        ),
        out_specs=(P("ep", "tp"), P("ep", "tp")),
        check_vma=False,
    )
```

profile of v0, /device:TPU:1, one launch (start us, length us, event | category | flops | bytes accessed | tf_op | source)
XLA Modules:
  0.0 256.7 jit_solution(7880721754247073453)
XLA Ops:
  7.2 0.0 copy-start
  7.2 0.0 all-gather.3.cloned.1.call-start
  7.2 0.7 broadcast_multiply_fusion
  8.0 0.8 copy.60
  8.8 0.1 eq.75
  8.9 0.1 eq.71
  9.0 1.2 fusion.25
  10.2 0.1 copy.59
  10.3 0.1 mul.144
  10.5 1.2 reduce-window.6
  11.6 0.2 slice_reduce_fusion
  11.9 0.1 fusion.46
  12.0 2.4 scatter_custom_fusion
  14.5 1.2 fusion.27
  15.8 0.0 copy-start.3
  15.8 0.0 copy-start.11
  15.8 0.0 copy-start.12
  15.8 0.0 copy-start.9
  15.8 0.0 copy-start.1
  15.8 6.0 %gather_fusion = bf16[1024,2048]{1,0:T(8,128)(2,1)} fusion(bf16[129,2048]{1,0:T(8,128)(2,1)S(1)} %concatenate.11, s32[1024]{0:T(1024)S(1)} %fusion.52), kind=kCustom, calls=%fused_computation | custom fusion | bytes 8392704 | tf_op jit(solution)/shard_map/gather | solution.py:146
  21.9 1.0 constant_dynamic-slice_fusion
  22.8 0.0 copy-start.2
  22.8 39.0 %all_to_all.21 = bf16[32,1,32,128]{3,2,1,0:T(8,128)(2,1)} all-to-all(bf16[32,1,32,128]{3,2,1,0:T(8,128)(2,1)S(1)} %constant_dynamic-slice_fusion), channel_id=1, replica_groups=mesh['ep'=32,'tp'=16] {'ep'}, dimensions={0} | all-to-all | bytes 524288 | tf_op jit(solution)/shard_map/all_to_all | solution.py:77
  61.9 0.0 all-gather.3.cloned.1.call-update
  61.9 0.0 copy-done.3
  61.9 0.2 fusion.22
  62.1 0.4 convolution_convert_fusion.1
  62.5 0.1 slice.89
  62.6 2.2 collective-permute-start
  64.9 0.8 collective-permute-done
  65.7 0.1 maximum_convert_fusion
  65.8 0.3 multiply_reduce_fusion
  66.0 0.6 broadcast_in_dim.61
  66.6 6.8 %all-to-all-start = ((f32[16,1,128]{2,1,0:T(1,128)}), f32[16,1,128]{2,1,0:T(1,128)S(1)}, u32[]{:S(2)}, u32[]{:S(2)}) async-start(f32[16,1,128]{2,1,0:T(1,128)} %broadcast_in_dim.61), calls=%async_computation | async-start | bytes 16384 | tf_op jit(solution)/shard_map/all_to_all | solution.py:31
  73.4 50.7 %all-gather.3.cloned.1.call-done = bf16[32,1,32,2048]{3,2,0,1:T(8,128)(2,1)} async-done(((bf16[32,1,32,128]{3,2,0,1:T(8,128)(2,1)}), bf16[32,1,32,2048]{3,2,0,1:T(8,128)(2,1)}) %all-gather.3.cloned.1.call-update) | async-done | bytes 4194320 | tf_op jit(solution)/shard_map/all_gather | solution.py:78
  124.1 3.4 %fusion.4 = f32[32,1,32,128]{3,2,0,1:T(8,128)S(1)} fusion(bf16[32,1,32,2048]{3,2,0,1:T(8,128)(2,1)} %all-gather.3.cloned.1.call-done, bf16[1,2048,128]{2,1,0:T(8,128)(2,1)S(1)} %copy-done.1), kind=kOutput, calls=%fused_computation.13 | convolution fusion | flops 536870912 | bytes 5242880 | tf_op jit(solution)/shard_map/send,edf->senf/dot_general | solution.py:79
  127.6 0.0 copy-done
  127.6 0.0 copy-done.2
  127.6 8.5 %convert_bitcast_fusion = bf16[1,32,4,16,8,128]{5,4,3,2,1,0:T(8,128)(2,1)} fusion(bf16[32,1,32,2048]{3,2,0,1:T(8,128)(2,1)} %all-gather.3.cloned.1.call-done, bf16[1,128,2048]{2,1,0:T(8,128)(2,1)S(1)} %copy-done, bf16[1,2048,128]{2,1,0:T(8,128)(2,1)S(1)} %copy-done.2, f32[32,1,32,128]{3,2,0,1:T(8,128)S(1)} %fusion.4), kind=kOutput, calls=%fused_computation.8 | convolution fusion | flops 1076625408 | bytes 9961472 | tf_op jit(solution)/shard_map/senf,efd->send/dot_general | solution.py:82
  136.1 5.2 %copy.73 = bf16[1,32,4,16,8,128]{5,4,2,1,0,3:T(8,128)(2,1)} copy(bf16[1,32,4,16,8,128]{5,4,3,2,1,0:T(8,128)(2,1)} %convert_bitcast_fusion) | data formatting | bytes 8388608 | tf_op jit(solution)/shard_map/reshape | solution.py:13
  141.3 0.0 all-to-all-done
  141.3 4.9 %all-to-all-start.2 = ((bf16[16,32,1,32,128]{4,3,1,2,0:T(8,128)(2,1)}), bf16[16,32,1,32,128]{4,3,1,2,0:T(8,128)(2,1)}, u32[]{:S(2)}, u32[]{:S(2)}) async-start(bf16[16,32,1,32,128]{4,3,1,2,0:T(8,128)(2,1)} %bitcast.117), calls=%async_computation.2 | async-start | bytes 8388608 | tf_op jit(solution)/shard_map/all_to_all | solution.py:19
  146.2 0.0 copy-start.8
  146.3 0.1 copy.66
  146.4 0.3 fusion.60
  146.7 0.3 fusion.20
  147.0 58.1 %all-to-all-done.2 = bf16[16,32,1,32,128]{4,3,1,2,0:T(8,128)(2,1)} async-done(((bf16[16,32,1,32,128]{4,3,1,2,0:T(8,128)(2,1)}), bf16[16,32,1,32,128]{4,3,1,2,0:T(8,128)(2,1)}, u32[]{:S(2)}, u32[]{:S(2)}) %all-to-all-start.2) | async-done | bytes 4194336 | tf_op jit(solution)/shard_map/all_to_all | solution.py:19
  205.1 3.5 %reduce_sum.85 = bf16[32,32,128]{2,1,0:T(8,128)(2,1)} reduce(bf16[16,32,1,32,128]{4,3,1,2,0:T(8,128)(2,1)} %all-to-all-done.2, bf16[]{:T(256)} %constant.90.clone.1), dimensions={0,2}, to_apply=%region_8.9 | reduce | flops 1966080 | bytes 4456450 | tf_op jit(solution)/shard_map/reduce_sum | solution.py:20
  208.6 15.7 %all-to-all-start.3 = ((bf16[32,1,32,128]{3,2,1,0:T(8,128)(2,1)}), bf16[32,1,32,128]{3,2,1,0:T(8,128)(2,1)S(1)}, u32[]{:S(2)}, u32[]{:S(2)}) async-start(bf16[32,1,32,128]{3,2,1,0:T(8,128)(2,1)} %bitcast.30), calls=%async_computation.3 | async-start | bytes 524288 | tf_op jit(solution)/shard_map/all_to_all | solution.py:84
  224.3 0.1 multiply_convert_fusion
  224.4 0.1 copy.57
  224.5 0.1 reshape.181
  224.6 20.2 %all-gather = bf16[393216]{0:T(1024)(128)(2,1)S(1)} all-gather(bf16[24576]{0:T(1024)(128)(2,1)S(1)} %pad_maximum_fusion), channel_id=2, replica_groups=mesh['ep'=32,'tp'=16] {'tp'}, dimensions={0}, use_global_device_ids=true | all-gather | bytes 835584 | tf_op jit(solution)/shard_map/all_gather | solution.py:46
  244.8 0.3 reshape.221
  245.3 0.1 copy.70
  245.4 0.3 copy.67
  245.6 0.5 reshape.183
  246.2 0.2 copy.58
  246.4 0.0 copy-done.6
  246.4 0.9 convolution_convert_fusion
  247.3 0.0 all-to-all-done.3
  247.3 1.3 gather_fusion.1
  248.7 0.2 fusion.42
  248.9 1.0 fusion.21
  (35 shorter events, 0.3 us)
Async XLA Ops:
  7.2 120.4 %copy-start = (bf16[1,128,2048]{2,1,0:T(8,128)(2,1)S(1)}, bf16[1,128,2048]{2,1,0:T(8,128)(2,1)}, u32[]{:S(2)}) copy-start(bf16[1,128,2048]{2,1,0:T(8,128)(2,1)} %param.28) | copy-start | bytes 1572868
  7.2 117.0 %all-gather.3.cloned.1.call-start = ((), (), s32[]{:S(2)}) async-start(), calls=%async_computation.4 | async-start | bytes 4456448 | tf_op jit(solution)/shard_map/all_gather | solution.py:78
  15.8 46.1 %copy-start.3 = (bf16[128,2048]{1,0:T(8,128)(2,1)S(1)}, bf16[128,2048]{1,0:T(8,128)(2,1)}, u32[]{:S(2)}) copy-start(bf16[128,2048]{1,0:T(8,128)(2,1)} %param.16) | copy-start | bytes 1572868
  15.8 46.3 %copy-start.11 = (bf16[2048,64]{0,1:T(8,128)(2,1)S(1)}, bf16[2048,64]{0,1:T(8,128)(2,1)}, u32[]{:S(2)}) copy-start(bf16[2048,64]{0,1:T(8,128)(2,1)} %param.20) | copy-start | bytes 786436
  15.8 46.3 %copy-start.12 = (f32[2048]{0:T(1024)S(1)}, f32[2048]{0:T(1024)}, u32[]{:S(2)}) copy-start(f32[2048]{0:T(1024)} %param.18) | copy-start | bytes 24580
  15.8 49.9 %copy-start.9 = (f32[64]{0:T(128)S(1)}, f32[64]{0:T(128)}, u32[]{:S(2)}) copy-start(f32[64]{0:T(128)} %param.21) | copy-start | bytes 772
  15.8 108.3 %copy-start.1 = (bf16[1,2048,128]{2,1,0:T(8,128)(2,1)S(1)}, bf16[1,2048,128]{2,1,0:T(8,128)(2,1)}, u32[]{:S(2)}) copy-start(bf16[1,2048,128]{2,1,0:T(8,128)(2,1)} %param.26) | copy-start | bytes 1572868
  22.8 104.7 %copy-start.2 = (bf16[1,2048,128]{2,1,0:T(8,128)(2,1)S(1)}, bf16[1,2048,128]{2,1,0:T(8,128)(2,1)}, u32[]{:S(2)}) copy-start(bf16[1,2048,128]{2,1,0:T(8,128)(2,1)} %param.27) | copy-start | bytes 1572868
  62.6 3.1 %collective-permute-start = (bf16[15,64]{0,1:T(8,128)(2,1)S(1)}, bf16[15,64]{0,1:T(8,128)(2,1)S(1)}, u32[]{:S(2)}, u32[]{:S(2)}) collective-permute-start(bf16[15,64]{0,1:T(8,128)(2,1)S(1)} %slice.89), channel_id=1, source_target_pairs={{0,16},{16,32},{32,48},{48,64},{64,80},{80,96},{96,112},{112,128},... | collective-permute-start | bytes 5768 | tf_op jit(solution)/shard_map/ppermute | solution.py:26
  66.6 74.7 %all-to-all-start = ((f32[16,1,128]{2,1,0:T(1,128)}), f32[16,1,128]{2,1,0:T(1,128)S(1)}, u32[]{:S(2)}, u32[]{:S(2)}) async-start(f32[16,1,128]{2,1,0:T(1,128)} %broadcast_in_dim.61), calls=%async_computation | async-start | bytes 16384 | tf_op jit(solution)/shard_map/all_to_all | solution.py:31
  141.3 4.9 %copy-start.7 = (f32[128,4]{0,1:T(4,128)S(1)}, f32[128,4]{0,1:T(4,128)}, u32[]{:S(2)}) copy-start(f32[128,4]{0,1:T(4,128)} %param.25) | copy-start | bytes 6148
  141.3 5.1 %copy-start.4 = (bf16[2048,128]{1,0:T(8,128)(2,1)S(1)}, bf16[2048,128]{1,0:T(8,128)(2,1)}, u32[]{:S(2)}) copy-start(bf16[2048,128]{1,0:T(8,128)(2,1)} %param.29) | copy-start | bytes 1572868
  141.3 5.4 %copy-start.10 = (bf16[2048,128]{1,0:T(8,128)(2,1)S(1)}, bf16[2048,128]{1,0:T(8,128)(2,1)}, u32[]{:S(2)}) copy-start(bf16[2048,128]{1,0:T(8,128)(2,1)} %param.30) | copy-start | bytes 1572868
  141.3 63.8 %all-to-all-start.2 = ((bf16[16,32,1,32,128]{4,3,1,2,0:T(8,128)(2,1)}), bf16[16,32,1,32,128]{4,3,1,2,0:T(8,128)(2,1)}, u32[]{:S(2)}, u32[]{:S(2)}) async-start(bf16[16,32,1,32,128]{4,3,1,2,0:T(8,128)(2,1)} %bitcast.117), calls=%async_computation.2 | async-start | bytes 8388608 | tf_op jit(solution)/shard_map/all_to_all | solution.py:19
  146.2 78.1 %copy-start.8 = (f32[64]{0:T(128)S(1)}, f32[64]{0:T(128)}, u32[]{:S(2)}) copy-start(f32[64]{0:T(128)} %param.22) | copy-start | bytes 772
  208.6 37.8 %copy-start.6 = (bf16[1024,128]{1,0:T(8,128)(2,1)S(1)}, bf16[1024,128]{1,0:T(8,128)(2,1)}, u32[]{:S(2)}) copy-start(bf16[1024,128]{1,0:T(8,128)(2,1)} %param.23) | copy-start | bytes 786436
  208.6 38.7 %all-to-all-start.3 = ((bf16[32,1,32,128]{3,2,1,0:T(8,128)(2,1)}), bf16[32,1,32,128]{3,2,1,0:T(8,128)(2,1)S(1)}, u32[]{:S(2)}, u32[]{:S(2)}) async-start(bf16[32,1,32,128]{3,2,1,0:T(8,128)(2,1)} %bitcast.30), calls=%async_computation.3 | async-start | bytes 524288 | tf_op jit(solution)/shard_map/all_to_all | solution.py:84
  244.8 4.1 %copy-start.5 = (bf16[2048,128]{1,0:T(8,128)(2,1)S(1)}, bf16[2048,128]{1,0:T(8,128)(2,1)}, u32[]{:S(2)}) copy-start(bf16[2048,128]{1,0:T(8,128)(2,1)} %param.31) | copy-start | bytes 1572868
Sparse Core Ops, SparseCore 0:
  62.0 62.0 all-gather.2
where the time goes:
time: 260 us; the launch traced here: 257 us
  waiting for transfers between devices  110 us (42%)
  blocking collectives  59.2 us (23%)
  starting transfers between devices  29.5 us (11%)
  local copies, waits for them, and re-layouts  20.1 us (8%)
  matrix products  14.7 us (6%)
  between operations  14.4 us (6%)
  other arithmetic  9.03 us (3%)
    all_to_all x1, waiting for transfers between devices, sum_at_owner(): lax.all_to_all(tiles, axis, split_axis=0, concat_axis=0, tiled=True)  58.1 us
    all_gather x1, waiting for transfers between devices, serve(): arrived = lax.all_gather(moved, 'tp', axis=3, tiled=True)  50.7 us
    all_to_all x1, blocking collectives, serve(): lax.all_to_all(own_part, 'ep', split_axis=0, concat_axis=0, tiled=True)  39 us
    all_gather x1, blocking collectives, gather_together(): lines, at, done = (lax.all_gather(ravelled, axis), 0, [])  20.2 us
    all_to_all x1, starting transfers between devices, serve(): return lax.all_to_all(summed, 'ep', split_axis=0, concat_axis=0, tiled=True)  15.7 us
    dot_general x1, matrix products, serve(): jnp.einsum('senf,efd->send', hidden, expert_down, preferred_element_type=...  8.5 us
    all_to_all x1, starting transfers between devices, copy_for_each(): return lax.all_to_all(copies, axis, split_axis=0, concat_axis=0, tiled=True)  6.75 us
    gather x1, local copies, waits for them, and re-layouts, on_device(): padded_rows[owner]  6.02 us
  transfers between devices with their start and end apart: 5, of which 3 were waited for; matrix products, arithmetic and copies ran while one was open for 9% of the time, Pallas kernels for 0%

commit v1 on v0

v1 whole, which is shorter than its diff:
```python
import functools

import jax
import jax.numpy as jnp
from jax import lax
from jax.experimental import pallas as pl
from jax.experimental.pallas import tpu as pltpu
from jax.sharding import PartitionSpec as P

MESH = pl.DeviceIdType.MESH
F32, BF16 = jnp.float32, jnp.bfloat16
EPS = 1e-06
SIDE = 4
LANES = 128


def dot(a, b):
    return jnp.dot(a, b, preferred_element_type=F32)


def silu_mul(gate, upper):
    return gate / (1.0 + jnp.exp(-gate)) * upper


class Sems:
    def __init__(self, send, recv):
        self.send, self.recv, self.used = send, recv, 0

    def take(self):
        at = self.used
        self.used += 1
        return self.send.at[at], self.recv.at[at]


def kernel(
    n_pairs,
    xe_ref, xm_hbm, mix_gain_ref, moe_gain_ref, pin_hbm, pscale_ref, pgain_ref, pout_hbm, route_ref, score_ref,
    eg_hbm, eu_hbm, ed_hbm, sg_hbm, su_hbm, sd_hbm,
    mix_out_ref, moe_out_ref,
    xm, wgu, wd, sgu, sd, pin, po2, mn, mm, sel, chi, clo, outgoing, x_all, part, q_a, q_b, y_own, back,
    opp1, main1, opp2, main2, halo_out, halo_in, sq_out, sq_in,
    load_sems, send_sems, recv_sems, z_send, z_recv, zb_send, zb_recv, sq_send, sq_recv,
):
    n_ep, n_tp = lax.axis_size("ep"), lax.axis_size("tp")
    ep, tp = lax.axis_index("ep"), lax.axis_index("tp")
    n_z = n_ep // 2
    z, core = ep // 2, ep % 2
    my, mx = tp // SIDE, tp % SIDE
    tok, width = xe_ref.shape
    rows_all = outgoing.shape[0]
    cap = rows_all // n_ep
    sems = Sems(send_sems, recv_sems)

    def slot_place(i):
        pair, other = i // 2, i % 2
        far = (pair + 1) // 2
        step = jnp.where(pair % 2 == 1, far, n_z - far)
        return step, other

    def peer_to(i):
        step, other = slot_place(i)
        return ((z + step) % n_z) * 2 + (core + other) % 2

    def peer_from(i):
        step, other = slot_place(i)
        return ((z + n_z - step) % n_z) * 2 + (core + other) % 2

    barrier = pltpu.get_barrier_semaphore()

    @pl.loop(1, n_ep)
    def _(i):
        pl.semaphore_signal(barrier, inc=1, device_id={"ep": (ep + i) % n_ep, "tp": tp}, device_id_type=MESH)

    @pl.loop(1, n_tp)
    def _(i):
        pl.semaphore_signal(barrier, inc=1, device_id={"ep": ep, "tp": (tp + i) % n_tp}, device_id_type=MESH)

    loads = {}
    for at, (name, src, dst) in enumerate((
        ("xm", xm_hbm, xm),
        ("pin", pin_hbm, pin),
        ("sg", sg_hbm, sgu.at[:, 0:LANES]),
        ("su", su_hbm, sgu.at[:, LANES:2 * LANES]),
        ("eg", eg_hbm.at[0], wgu.at[:, 0:LANES]),
        ("eu", eu_hbm.at[0], wgu.at[:, LANES:2 * LANES]),
        ("ed", ed_hbm.at[0], wd),
        ("po_a", pout_hbm, po2.at[:, 0]),
        ("po_b", pout_hbm, po2.at[:, 1]),
        ("sd", sd_hbm, sd),
    )):
        loads[name] = pltpu.make_async_copy(src, dst, load_sems.at[at])
        loads[name].start()

    def row_norm(src, gain_ref, dst):
        @pl.loop(0, tok // 16)
        def _(b):
            at = pl.ds(pl.multiple_of(b * 16, 16), 16)
            values = src[at, :].astype(F32)
            scale = lax.rsqrt(jnp.mean(values * values, axis=-1, keepdims=True) + EPS)
            dst[at, :] = (values * scale * gain_ref[...]).astype(BF16)

    row_norm(xe_ref, moe_gain_ref, mn)

    top = route_ref.shape[1]
    lane = lax.broadcasted_iota(jnp.int32, (tok, LANES), 1)
    table = jnp.zeros((tok, LANES), F32)
    for k in range(top):
        table = jnp.where(lane == k, route_ref[:, k:k + 1].astype(F32), table)
        table = jnp.where(lane == top + k, score_ref[:, k:k + 1], table)
    table = table.T
    slot_i = lax.broadcasted_iota(jnp.int32, (n_ep, tok), 0)
    pair_i, other_i = slot_i // 2, slot_i % 2
    far_i = (pair_i + 1) // 2
    step_i = jnp.where(pair_i % 2 == 1, far_i, n_z - far_i)
    expert_i = (((z + step_i) % n_z) * 2 + (core + other_i) % 2).astype(F32)
    total = table[top:top + 1, :]
    for k in range(1, top):
        total = total + table[top + k:top + k + 1, :]
    hit = jnp.zeros((n_ep, tok), F32)
    weight = jnp.zeros((n_ep, tok), F32)
    for k in range(top):
        same = expert_i == table[k:k + 1, :]
        hit = jnp.where(same, 1.0, hit)
        weight = jnp.where(same, 2.5 * table[top + k:top + k + 1, :] / total, weight)
    before = (
        lax.broadcasted_iota(jnp.int32, (tok, tok), 0) < lax.broadcasted_iota(jnp.int32, (tok, tok), 1)
    )
    rank = dot(hit.astype(BF16), jnp.where(before, 1.0, 0.0).astype(BF16))
    place = jnp.where(hit > 0.0, rank, -1.0)
    slot_row = lax.broadcasted_iota(jnp.int32, (cap, tok), 0).astype(F32)
    for i in range(n_ep):
        sel[i * cap:(i + 1) * cap, :] = jnp.where(place[i:i + 1, :] == slot_row, 1.0, 0.0).astype(BF16)

    share = mn[:, pl.ds(pl.multiple_of(tp * LANES, LANES), LANES)]
    outgoing[...] = dot(sel[...], share).astype(BF16)
    x_all[my, mx, 0:cap, :] = outgoing[0:cap, :]

    pl.semaphore_wait(barrier, n_ep - 1 + n_tp - 1)

    per_chunk = n_ep // (2 * n_pairs)

    @pl.loop(1, n_ep)
    def _(i):
        at = pl.ds(pl.multiple_of(i * cap, cap), cap)
        pltpu.make_async_remote_copy(
            src_ref=outgoing.at[at], dst_ref=x_all.at[my, mx, at], send_sem=z_send, recv_sem=z_recv.at[i // per_chunk],
            device_id={"ep": peer_to(i), "tp": tp}, device_id_type=MESH,
        ).start()

    loads["xm"].wait()
    row_norm(xm, mix_gain_ref, mm)
    loads["pin"].wait()
    narrow = pin.shape[1]
    pooled_in = dot(mm[...], pin[...])
    pooled_in = jnp.concatenate([pooled_in, jnp.zeros((tok, LANES - narrow), F32)], axis=1).astype(BF16)
    halo_out[...] = pooled_in[tok - 16:, :]
    halo_sem = sems.take()
    halo = pltpu.make_async_remote_copy(
        src_ref=halo_out, dst_ref=halo_in, send_sem=halo_sem[0], recv_sem=halo_sem[1],
        device_id={"ep": (ep + 1) % n_ep, "tp": tp}, device_id_type=MESH,
    )
    halo.start()

    loads["sg"].wait()
    loads["su"].wait()
    both = dot(mn[...], sgu[...])
    shared_rows = slice(rows_all, rows_all + tok)
    x_all[my, mx, shared_rows, :] = silu_mul(both[:, :LANES], both[:, LANES:]).astype(BF16)

    def copy(src, dst, where):
        send, recv = sems.take()
        made = pltpu.make_async_remote_copy(
            src_ref=src, dst_ref=dst, send_sem=send, recv_sem=recv, device_id=where, device_id_type=MESH
        )
        sent.append(made)
        return made

    sent = [halo]
    x_ring = lambda step: {"ep": ep, "tp": my * SIDE + (mx + step) % SIDE}
    y_ring = lambda step: {"ep": ep, "tp": ((my + step) % SIDE) * SIDE + mx}

    class Ring:
        def __init__(self, view, me, ring, start, count):
            self.view, self.me, self.ring, self.start_row, self.count = view, me, ring, start, count

        def unit(self, step, part=None):
            half = self.count // 2
            lo, n = {None: (0, self.count), 0: (0, half), 1: (half, half)}[part]
            return self.view((self.me + step) % SIDE, pl.ds(self.start_row + lo, n))

        def start(self):
            own = self.unit(0)
            self.right = copy(own, own, self.ring(1))
            self.left = copy(own, own, self.ring(SIDE - 1))
            self.right.start()
            self.left.start()

        def relay(self):
            first, second = self.unit(SIDE - 1, 0), self.unit(1, 1)
            self.right.wait_recv()
            self.on_right = copy(first, first, self.ring(1))
            self.on_right.start()
            self.left.wait_recv()
            self.on_left = copy(second, second, self.ring(SIDE - 1))
            self.on_left.start()

        def finish(self):
            self.on_right.wait_recv()
            self.on_left.wait_recv()

    class Gather:
        def __init__(self, start, count, x_first):
            along_x = lambda i, at: x_all.at[my, i, at]
            along_y = lambda i, at: x_all.at[i, mx, at]
            whole_y = lambda i, at: x_all.at[i, :, at]
            whole_x = lambda i, at: x_all.at[:, i, at]
            if x_first:
                self.one = Ring(along_x, mx, x_ring, start, count)
                self.two = Ring(whole_y, my, y_ring, start, count)
            else:
                self.one = Ring(along_y, my, y_ring, start, count)
                self.two = Ring(whole_x, mx, x_ring, start, count)

    def gather_pair(a, b):
        return Gather(*a, True), Gather(*b, False)

    shared_gather = Gather(rows_all, tok, True)
    shared_gather.one.start()

    halo.wait_recv()
    carried = jnp.where(ep > 0, halo_in[...].astype(F32), 0.0)
    ext = jnp.concatenate([carried, pooled_in.astype(F32)], axis=0)
    sums, chosen, window = ext, None, 1
    for index in range(4):
        sums = sums + pltpu.roll(sums, window, 0)
        window *= 2
        chosen = sums if chosen is None else jnp.where(my >= index, sums, chosen)
    position = (ep * tok + lax.broadcasted_iota(jnp.int32, (tok, LANES), 0) + 1).astype(F32)
    widest = lax.shift_left(2, my).astype(F32)
    zeros_right = jnp.zeros((1, LANES - narrow), F32)
    pscale = jnp.concatenate([pscale_ref[...], zeros_right], axis=1)
    pgain = jnp.concatenate([pgain_ref[...], zeros_right], axis=1)
    scaled = (chosen[16:, :] / jnp.minimum(position, widest) - pooled_in.astype(F32)) * pscale
    squares = jnp.sum(scaled * scaled, axis=1, keepdims=True)
    squares = jnp.broadcast_to(squares, (tok, LANES)).T[0:8, :]
    sq_out[...] = squares

    @pl.loop(1, n_tp)
    def _(i):
        pltpu.make_async_remote_copy(
            src_ref=sq_out, dst_ref=sq_in.at[i - 1], send_sem=sq_send, recv_sem=sq_recv,
            device_id={"ep": ep, "tp": (tp + i) % n_tp}, device_id_type=MESH,
        ).start()

    high = weight.astype(BF16).astype(F32)
    low = weight - high
    for i in range(n_ep):
        at = slice(i * cap, (i + 1) * cap)
        same = place[i:i + 1, :] == slot_row
        chi[at, :] = jnp.where(same, high[i:i + 1, :], 0.0).astype(BF16)
        clo[at, :] = jnp.where(same, low[i:i + 1, :], 0.0).astype(BF16)

    shared_gather.one.relay()
    pltpu.make_async_copy(sq_in, sq_in, sq_recv).wait()
    for i in range(n_tp - 1):
        squares = squares + sq_in[i]
    squares = jnp.broadcast_to(squares[0:1, :], (tok, LANES)).T
    pooled = (scaled * lax.rsqrt(squares / (narrow * n_tp) + EPS) * pgain).astype(BF16).astype(F32)
    packed = pooled[:tok // 2, :] + pltpu.roll(pooled[tok // 2:, :], narrow, 1)
    pool_start = rows_all + tok
    x_all[my, mx, pool_start:pool_start + tok // 2, :] = packed.astype(BF16)
    pool_gather = Gather(pool_start, tok // 2, False)
    pool_gather.one.start()
    shared_gather.one.finish()
    shared_gather.two.start()
    pool_gather.one.relay()
    pool_gather.one.finish()
    pool_gather.two.start()

    loads["eg"].wait()
    loads["eu"].wait()
    loads["ed"].wait()

    count = rows_all // (2 * n_pairs)
    half = count // 2

    class RingSum:
        def __init__(self, view, me, ring, opp, main, start):
            self.view, self.me, self.ring, self.opp, self.main, self.start_row = view, me, ring, opp, main, start

        def unit(self, step, part):
            lo, n = {None: (0, count), 0: (0, half), 1: (half, half)}[part]
            return self.view((self.me + step) % SIDE, pl.ds(self.start_row + lo, n))

        def into(self, side, part):
            at = pl.ds(part * half, half)
            return self.main.at[(side,) + (slice(None),) * (len(self.main.shape) - 3) + (at,)]

        def start(self):
            self.opp_right = copy(self.unit(2, 0), self.opp.at[0], self.ring(1))
            self.opp_left = copy(self.unit(2, 1), self.opp.at[1], self.ring(SIDE - 1))
            self.far_right = copy(self.unit(1, 1), self.into(0, 1), self.ring(1))
            self.far_left = copy(self.unit(SIDE - 1, 0), self.into(1, 0), self.ring(SIDE - 1))
            for made in (self.opp_right, self.opp_left, self.far_right, self.far_left):
                made.start()

        def add(self, unit, extra):
            unit[...] = (unit[...].astype(F32) + extra[...].astype(F32)).astype(BF16)

        def relay(self):
            self.opp_right.wait_recv()
            self.add(self.unit(1, 0), self.opp.at[0])
            self.near_right = copy(self.unit(1, 0), self.into(0, 0), self.ring(1))
            self.near_right.start()
            self.opp_left.wait_recv()
            self.add(self.unit(SIDE - 1, 1), self.opp.at[1])
            self.near_left = copy(self.unit(SIDE - 1, 1), self.into(1, 1), self.ring(SIDE - 1))
            self.near_left.start()

        def finish(self, dst):
            for made in (self.far_right, self.far_left, self.near_right, self.near_left):
                made.wait_recv()
            own = self.unit(0, None)
            dst[...] = (own[...].astype(F32) + self.main[0].astype(F32) + self.main[1].astype(F32)).astype(BF16)

    tile = min(256, count)

    def experts(start, rows):
        @pl.loop(0, rows // tile)
        def _(b):
            at = pl.ds(pl.multiple_of(start + b * tile, tile), tile)
            lhs = jnp.concatenate([x_all[i // SIDE, i % SIDE, at, :] for i in range(n_tp)], axis=1)
            pair = dot(lhs, wgu[...])
            hidden = silu_mul(pair[:, :LANES], pair[:, LANES:]).astype(BF16)
            for j in range(n_tp // 2):
                out = dot(hidden, wd[:, j * 2 * LANES:(j + 1) * 2 * LANES])
                for s in range(2):
                    i = 2 * j + s
                    part[i // SIDE, i % SIDE, at, :] = out[:, s * LANES:(s + 1) * LANES].astype(BF16)

    class Pair:
        def __init__(self, k):
            self.k = k
            self.a_start, self.b_start = 2 * k * count, (2 * k + 1) * count
            self.gathers = gather_pair((self.a_start, count), (self.b_start, count))
            one = (
                RingSum(lambda i, at: part.at[i, :, at], my, y_ring, opp1.at[0, k], main1.at[0, k], self.a_start),
                RingSum(lambda i, at: part.at[:, i, at], mx, x_ring, opp1.at[1, k], main1.at[1, k], self.b_start),
            )
            two = (
                RingSum(lambda i, at: q_a.at[k, i, at], mx, x_ring, opp2.at[0, k], main2.at[0, k], 0),
                RingSum(lambda i, at: q_b.at[k, i, at], my, y_ring, opp2.at[1, k], main2.at[1, k], 0),
            )
            self.sums = (one, two)

        def arrive(self):
            for chunk in (2 * self.k, 2 * self.k + 1):
                lo = cap if chunk == 0 else chunk * count
                got = x_all.at[my, mx, pl.ds(lo, (chunk + 1) * count - lo)]
                pltpu.make_async_copy(got, got, z_recv.at[chunk]).wait()

        def gather(self, phase, step):
            for g in self.gathers:
                getattr((g.one, g.two)[phase], step)()

        def compute(self):
            experts(self.a_start, 2 * count)

        def sum(self, phase, step):
            for s in self.sums[phase]:
                getattr(s, step)()

        def middle(self):
            self.sums[0][0].finish(q_a.at[self.k])
            self.sums[0][1].finish(q_b.at[self.k])

        def close(self):
            self.sums[1][0].finish(y_own.at[pl.ds(self.a_start, count)])
            self.sums[1][1].finish(y_own.at[pl.ds(self.b_start, count)])
            first = self.a_start // cap
            if first == 0:
                back[0:cap, :] = y_own[0:cap, :]

            @pl.loop(max(first, 1), first + 2 * count // cap)
            def _(i):
                at = pl.ds(pl.multiple_of(i * cap, cap), cap)
                pltpu.make_async_remote_copy(
                    src_ref=y_own.at[at], dst_ref=back.at[at], send_sem=zb_send, recv_sem=zb_recv,
                    device_id={"ep": peer_from(i), "tp": tp}, device_id_type=MESH,
                ).start()

    pairs = [Pair(k) for k in range(n_pairs)]
    last = n_pairs - 1

    for k, p in enumerate(pairs):
        p.arrive()
        p.gather(0, "start")
        p.gather(0, "relay")
        p.gather(0, "finish")
        p.gather(1, "start")
        if k == 0:
            shared_gather.two.relay()
            pool_gather.two.relay()
        else:
            pairs[k - 1].gather(1, "relay")
    for k, p in enumerate(pairs):
        if k == last:
            p.gather(1, "relay")
        p.gather(1, "finish")
        p.compute()
        p.sum(0, "start")
        if k > 0:
            pairs[k - 1].sum(0, "relay")
    for k, p in enumerate(pairs):
        if k == last:
            p.sum(0, "relay")
        p.middle()
        p.sum(1, "start")
        if k > 0:
            pairs[k - 1].sum(1, "relay")
            pairs[k - 1].close()
    pairs[last].sum(1, "relay")
    pairs[last].close()

    shared_gather.two.finish()
    pool_gather.two.finish()
    for name in ("po_a", "po_b", "sd"):
        loads[name].wait()
    lane = lax.broadcasted_iota(jnp.int32, (tok // 2, LANES), 1)
    zero = jnp.zeros((tok // 2, LANES), BF16)
    upper, lower = [], []
    for i in range(n_tp):
        block = x_all[i // SIDE, i % SIDE, pool_start:pool_start + tok // 2, :]
        upper.append(jnp.where(lane < narrow, block, zero))
        lower.append(jnp.where(lane < narrow, zero, block))
    lhs = jnp.concatenate([jnp.concatenate(upper, axis=1), jnp.concatenate(lower, axis=1)], axis=0)
    mix_out_ref[...] = dot(lhs, po2[...].reshape(2 * n_tp * narrow, LANES)).astype(BF16)
    lhs = jnp.concatenate([x_all[i // SIDE, i % SIDE, shared_rows, :] for i in range(n_tp)], axis=1)
    result = dot(lhs, sd[...])

    arrived = back.at[pl.ds(cap, rows_all - cap)]
    pltpu.make_async_copy(arrived, arrived, zb_recv).wait()
    over = (((0,), (0,)), ((), ()))
    result += lax.dot_general(chi[...], back[...], over, preferred_element_type=F32)
    result += lax.dot_general(clo[...], back[...], over, preferred_element_type=F32)
    moe_out_ref[...] = result.astype(BF16)

    for made in sent:
        made.wait_send()
    for whole, sem in ((outgoing, z_send), (y_own, zb_send)):
        gone = whole.at[pl.ds(cap, rows_all - cap)]
        pltpu.make_async_copy(gone, gone, sem).wait()
    pltpu.make_async_copy(sq_in, sq_in, sq_send).wait()


def on_device(n_pairs, mix_input, expert_input, mix_gain, moe_gain, pool_in, pool_scale, pool_gain, pool_out, route,
              route_score, expert_gate, expert_up, expert_down, shared_gate, shared_up, shared_down):
    n_ep, n_tp = lax.axis_size("ep"), lax.axis_size("tp")
    tok, width = mix_input.shape
    top = route.shape[1]
    cap = 2 * tok * top // n_ep
    rows = cap * n_ep
    narrow = pool_in.shape[1]
    count = rows // (2 * n_pairs)
    everything = rows + tok + tok // 2
    vmem = pl.BlockSpec(memory_space=pltpu.VMEM)
    hbm = pl.BlockSpec(memory_space=pltpu.HBM)
    dma = pltpu.SemaphoreType.DMA
    n_copies = 1 + 16 + n_pairs * 40
    return pl.pallas_call(
        functools.partial(kernel, n_pairs),
        out_shape=(
            jax.ShapeDtypeStruct((tok, pool_out.shape[1]), BF16),
            jax.ShapeDtypeStruct((tok, shared_down.shape[1]), BF16),
        ),
        in_specs=[vmem, hbm, vmem, vmem, hbm, vmem, vmem, hbm, vmem, vmem, hbm, hbm, hbm, hbm, hbm, hbm],
        out_specs=(vmem, vmem),
        scratch_shapes=[
            pltpu.VMEM((tok, width), BF16),
            pltpu.VMEM((width, 2 * LANES), BF16),
            pltpu.VMEM((LANES, width), BF16),
            pltpu.VMEM((width, 2 * LANES), BF16),
            pltpu.VMEM((width, LANES), BF16),
            pltpu.VMEM((width, narrow), BF16),
            pltpu.VMEM((n_tp, 2, narrow, LANES), BF16),
            pltpu.VMEM((tok, width), BF16),
            pltpu.VMEM((tok, width), BF16),
            pltpu.VMEM((rows, LANES), BF16),
            pltpu.VMEM((rows, LANES), BF16),
            pltpu.VMEM((rows, LANES), BF16),
            pltpu.VMEM((rows, LANES), BF16),
            pltpu.VMEM((SIDE, SIDE, everything, LANES), BF16),
            pltpu.VMEM((SIDE, SIDE, rows, LANES), BF16),
            pltpu.VMEM((n_pairs, SIDE, count, LANES), BF16),
            pltpu.VMEM((n_pairs, SIDE, count, LANES), BF16),
            pltpu.VMEM((rows, LANES), BF16),
            pltpu.VMEM((rows, LANES), BF16),
            pltpu.VMEM((2, n_pairs, 2, SIDE, count // 2, LANES), BF16),
            pltpu.VMEM((2, n_pairs, 2, SIDE, count, LANES), BF16),
            pltpu.VMEM((2, n_pairs, 2, count // 2, LANES), BF16),
            pltpu.VMEM((2, n_pairs, 2, count, LANES), BF16),
            pltpu.VMEM((16, LANES), BF16),
            pltpu.VMEM((16, LANES), BF16),
            pltpu.VMEM((8, LANES), F32),
            pltpu.VMEM((n_tp - 1, 8, LANES), F32),
            dma((10,)),
            dma((n_copies,)),
            dma((n_copies,)),
            dma,
            dma((2 * n_pairs,)),
            dma,
            dma,
            dma,
            dma,
        ],
        compiler_params=pltpu.CompilerParams(
            collective_id=0, has_side_effects=True, vmem_limit_bytes=60 * 1024 * 1024
        ),
    )(
        expert_input,
        mix_input,
        mix_gain.reshape(1, -1),
        moe_gain.reshape(1, -1),
        pool_in,
        pool_scale.reshape(1, -1),
        pool_gain.reshape(1, -1),
        pool_out.reshape(n_tp, narrow, pool_out.shape[1]),
        route,
        route_score,
        expert_gate,
        expert_up,
        expert_down,
        shared_gate,
        shared_up,
        shared_down,
    )


def solution(mesh):
    return jax.shard_map(
        functools.partial(on_device, 2),
        mesh=mesh,
        in_specs=(
            P("ep", None),
            P("ep", None),
            P(),
            P(),
            P(None, "tp"),
            P("tp"),
            P("tp"),
            P(None, "tp"),
            P("ep", None),
            P("ep", None),
            P("ep", None, "tp"),
            P("ep", None, "tp"),
            P("ep", "tp", None),
            P(None, "tp"),
            P(None, "tp"),
            P(None, "tp"),
        ),
        out_specs=(P("ep", "tp"), P("ep", "tp")),
        check_vma=False,
    )
```

time: 260 us -> 129 us (0.50); the launches traced: 257 us -> 129 us
  Pallas kernels: 0 us -> 122 us
  waiting for transfers between devices: 110 us -> 0 us
  blocking collectives: 59.2 us -> 0 us
  starting transfers between devices: 29.5 us -> 0 us
  matrix products: 14.7 us -> 0 us
  local copies, waits for them, and re-layouts: 20.1 us -> 6.08 us
  between operations: 14.4 us -> 0.66 us
  other arithmetic: 9.03 us -> 0 us
    pallas_call x0 -> x1, Pallas kernels: none -> 122 us  [on_device(): pl.pallas_call(functools.partial(kernel, n_pairs), out_shape=(jax.ShapeDt...]
    all_to_all x3 -> x0, waiting for transfers between devices: 58.1 us -> none  [the longest x1 58.1 us: sum_at_owner(): lax.all_to_all(tiles, axis, split_axis=0, concat_axis=0, tiled=True)]
    all_gather x1 -> x0, waiting for transfers between devices: 50.7 us -> none  [serve(): arrived = lax.all_gather(moved, 'tp', axis=3, tiled=True)]
    all_to_all x1 -> x0, blocking collectives: 39 us -> none  [serve(): lax.all_to_all(own_part, 'ep', split_axis=0, concat_axis=0, tiled=True)]
    all_to_all x3 -> x0, starting transfers between devices: 27.3 us -> none  [the longest x1 15.7 us: serve(): return lax.all_to_all(summed, 'ep', split_axis=0, concat_axis=0, tiled=True)]
    all_gather x1 -> x0, blocking collectives: 20.2 us -> none  [gather_together(): lines, at, done = (lax.all_gather(ravelled, axis), 0, [])]
    dot_general x7 -> x0, matrix products: 14.7 us -> none  [the longest x1 8.5 us: serve(): jnp.einsum('senf,efd->send', hidden, expert_down, preferred_element_type=...]
    gather x2 -> x0, local copies, waits for them, and re-layouts: 7.35 us -> none  [the longest x1 6.02 us: on_device(): padded_rows[owner]]
  transfers between devices with their start and end apart: 5 -> 0, of which waited for: 3 -> 0; matrix products, arithmetic and copies ran while one was open for 9% -> 0% of each run, Pallas kernels for 0% -> 0%
where the time goes in v1:
time: 129 us
  Pallas kernels  122 us (95%)
  local copies, waits for them, and re-layouts  6.08 us (5%)
    pallas_call x1, Pallas kernels, on_device(): pl.pallas_call(functools.partial(kernel, n_pairs), out_shape=(jax.ShapeDt...  122 us
    unnamed x11, local copies, waits for them, and re-layouts  6.08 us

profile of v1, /device:TPU:1, one launch (start us, length us, event | category | flops | bytes accessed | tf_op | source)
XLA Modules:
  0.0 129.2 jit_solution(11225707142306633761)
XLA Ops:
  0.6 0.0 copy-start.1
  0.6 0.7 copy-done.1
  1.3 0.0 copy-start.2
  1.3 0.7 copy.19.route_ref
  2.0 0.0 copy-done.2
  2.0 0.7 copy.20.score_ref
  2.8 1.9 %copy.18.pin_hbm = bf16[2048,64]{1,0:T(8,128)(2,1)} copy(bf16[2048,64]{0,1:T(8,128)(2,1)} %param.20) | data formatting | bytes 524288 | tf_op args[4]
  4.7 122.4 %shard_map.167 = (bf16[128,128]{1,0:T(8,128)(2,1)}, bf16[128,128]{1,0:T(8,128)(2,1)}) custom-call(bf16[128,2048]{1,0:T(8,128)(2,1)} %xe_ref.1, bf16[128,2048]{1,0:T(8,128)(2,1)} %xm_hbm.1, f32[1,2048]{1,0:T(1,128)} %bitcast.6, f32[1,2048]{1,0:T(1,128)} %bitcast.7, bf16[2048,64]{1,0:T(8,128)(2,1)} %copy.18.pin_hbm, f32[1,64]{1,0:T(1,128)} %bitcast.8, ...), custom_call_target="tpu_custom_call" | custom-call | tf_op jit(solution)/shard_map/pallas_call | solution.py:470
  127.1 0.0 copy-start
  127.2 1.4 %copy.23 = bf16[128,128]{1,0:T(8,128)(2,1)} copy(bf16[128,128]{1,0:T(8,128)(2,1)} %get-tuple-element.4) | data formatting | bytes 65536
  128.5 0.0 copy-done
  128.5 0.6 copy.24
Async XLA Ops:
  0.6 0.7 copy-start.1
  1.3 0.7 copy-start.2
  127.1 1.4 %copy-start = (bf16[128,128]{1,0:T(8,128)(2,1)S(1)}, bf16[128,128]{1,0:T(8,128)(2,1)}, u32[]{:S(2)}) copy-start(bf16[128,128]{1,0:T(8,128)(2,1)} %get-tuple-element.5) | copy-start | bytes 98308

commit v2 on v1

v2 whole, which is shorter than its diff:
```python
import functools
import math

import jax
import jax.numpy as jnp
from jax import lax
from jax.experimental import pallas as pl
from jax.experimental.pallas import tpu as pltpu
from jax.sharding import PartitionSpec as P

MESH = pl.DeviceIdType.MESH
F32, BF16 = jnp.float32, jnp.bfloat16
EPS = 1e-06
SIDE = 4
LANES = 128


def dot(a, b):
    return jnp.dot(a, b, preferred_element_type=F32)


def silu_mul(gate, upper):
    return gate / (1.0 + jnp.exp(-gate)) * upper


class Sems:
    def __init__(self, recv):
        self.recv, self.used = recv, 0

    def take(self):
        at = self.used
        self.used += 1
        return self.recv.at[at]


def kernel(
    n_pairs,
    xe_hbm, xm_hbm, mix_gain_ref, moe_gain_ref, pin_hbm, pscale_ref, pgain_ref, pout_hbm, route_ref, score_ref,
    eg_hbm, eu_hbm, ed_hbm, sg_hbm, su_hbm, sd_hbm,
    mix_out_ref, moe_out_ref,
    xe, xm, wgu, wd, sgu, sd, pin, po2, mn, mm, sel, chi, clo, outgoing, x_all, part, q_a, q_b, y_own, back,
    opp1, main1, opp2, main2, halo_out, halo_in, sq_out, sq_in,
    load_sems, send_sems, recv_sems, z_send, z_recv, zb_send, zb_recv, sq_send, sq_recv,
):
    n_ep, n_tp = lax.axis_size("ep"), lax.axis_size("tp")
    ep, tp = lax.axis_index("ep"), lax.axis_index("tp")
    n_z = n_ep // 2
    z, core = ep // 2, ep % 2
    my, mx = tp // SIDE, tp % SIDE
    tok, width = xe_hbm.shape
    rows_all = outgoing.shape[0]
    cap = rows_all // n_ep
    sems = Sems(recv_sems)

    def slot_place(i):
        pair, other = i // 2, i % 2
        far = (pair + 1) // 2
        step = jnp.where(pair % 2 == 1, far, n_z - far)
        return step, other

    def peer_to(i):
        step, other = slot_place(i)
        return ((z + step) % n_z) * 2 + (core + other) % 2

    def peer_from(i):
        step, other = slot_place(i)
        return ((z + n_z - step) % n_z) * 2 + (core + other) % 2

    loads = {}

    def load(name, src, dst):
        loads[name] = pltpu.make_async_copy(src, dst, load_sems.at[len(loads)])
        loads[name].start()

    load("xe", xe_hbm, xe)

    barrier = pltpu.get_barrier_semaphore()

    @pl.loop(1, n_ep)
    def _(i):
        pl.semaphore_signal(barrier, inc=1, device_id={"ep": (ep + i) % n_ep, "tp": tp}, device_id_type=MESH)

    @pl.loop(1, n_tp)
    def _(i):
        pl.semaphore_signal(barrier, inc=1, device_id={"ep": ep, "tp": (tp + i) % n_tp}, device_id_type=MESH)

    load("xm", xm_hbm, xm)
    load("pin", pin_hbm, pin)
    load("sg", sg_hbm, sgu.at[:, 0:LANES])
    load("su", su_hbm, sgu.at[:, LANES:2 * LANES])
    load("eg", eg_hbm.at[0], wgu.at[:, 0:LANES])
    load("eu", eu_hbm.at[0], wgu.at[:, LANES:2 * LANES])
    load("ed", ed_hbm.at[0], wd)
    load("po_a", pout_hbm, po2.at[:, 0])
    load("po_b", pout_hbm, po2.at[:, 1])
    load("sd", sd_hbm, sd)

    def row_norm(src, gain_ref, dst):
        @pl.loop(0, tok // 16)
        def _(b):
            at = pl.ds(pl.multiple_of(b * 16, 16), 16)
            values = src[at, :].astype(F32)
            scale = lax.rsqrt(jnp.mean(values * values, axis=-1, keepdims=True) + EPS)
            dst[at, :] = (values * scale * gain_ref[...]).astype(BF16)


    top = route_ref.shape[0]
    routes = [route_ref[k:k + 1, :].astype(F32) for k in range(top)]
    scores = [score_ref[k:k + 1, :] for k in range(top)]
    slot_i = lax.broadcasted_iota(jnp.int32, (n_ep, tok), 0)
    pair_i, other_i = slot_i // 2, slot_i % 2
    far_i = (pair_i + 1) // 2
    step_i = jnp.where(pair_i % 2 == 1, far_i, n_z - far_i)
    expert_i = (((z + step_i) % n_z) * 2 + (core + other_i) % 2).astype(F32)
    total = scores[0]
    for k in range(1, top):
        total = total + scores[k]
    hit = jnp.zeros((n_ep, tok), F32)
    weight = jnp.zeros((n_ep, tok), F32)
    for k in range(top):
        same = expert_i == routes[k]
        hit = jnp.where(same, 1.0, hit)
        weight = jnp.where(same, 2.5 * scores[k] / total, weight)
    before = (
        lax.broadcasted_iota(jnp.int32, (tok, tok), 0) < lax.broadcasted_iota(jnp.int32, (tok, tok), 1)
    )
    rank = dot(hit.astype(BF16), jnp.where(before, 1.0, 0.0).astype(BF16))
    place = jnp.where(hit > 0.0, rank, -1.0)
    slot_row = lax.broadcasted_iota(jnp.int32, (cap, tok), 0).astype(F32)
    for i in range(n_ep):
        sel[i * cap:(i + 1) * cap, :] = jnp.where(place[i:i + 1, :] == slot_row, 1.0, 0.0).astype(BF16)

    loads["xe"].wait()
    row_norm(xe, moe_gain_ref, mn)
    share = mn[:, pl.ds(pl.multiple_of(tp * LANES, LANES), LANES)]
    outgoing[...] = dot(sel[...], share).astype(BF16)
    x_all[my, mx, 0:cap, :] = outgoing[0:cap, :]

    pl.semaphore_wait(barrier, n_ep - 1 + n_tp - 1)

    near = n_pairs // 4
    order = list(range(near)) + list(range(2 * near, n_pairs)) + list(range(2 * near - 1, near - 1, -1))
    per_pair = n_ep // n_pairs
    for k in order:

        @pl.loop(max(1, k * per_pair), (k + 1) * per_pair)
        def _(i):
            at = pl.ds(pl.multiple_of(i * cap, cap), cap)
            pltpu.make_async_remote_copy(
                src_ref=outgoing.at[at], dst_ref=x_all.at[my, mx, at], send_sem=z_send, recv_sem=z_recv.at[k],
                device_id={"ep": peer_to(i), "tp": tp}, device_id_type=MESH,
            ).start()

    def copy(src, dst, where, group):
        send_all[group] += math.prod(src.shape)
        return pltpu.make_async_remote_copy(
            src_ref=src, dst_ref=dst, send_sem=send_sems.at[group], recv_sem=sems.take(),
            device_id=where, device_id_type=MESH,
        )

    send_all = [0] * (n_pairs + 3)
    x_ring = lambda step: {"ep": ep, "tp": my * SIDE + (mx + step) % SIDE}
    y_ring = lambda step: {"ep": ep, "tp": ((my + step) % SIDE) * SIDE + mx}

    class Ring:
        def __init__(self, view, me, ring, start, count, group):
            self.view, self.me, self.ring, self.start_row, self.count = view, me, ring, start, count
            self.group = group

        def unit(self, step, part=None):
            half = self.count // 2
            lo, n = {None: (0, self.count), 0: (0, half), 1: (half, half)}[part]
            return self.view((self.me + step) % SIDE, pl.ds(self.start_row + lo, n))

        def start(self):
            own = self.unit(0)
            self.right = copy(own, own, self.ring(1), self.group)
            self.left = copy(own, own, self.ring(SIDE - 1), self.group)
            self.right.start()
            self.left.start()

        def relay(self):
            first, second = self.unit(SIDE - 1, 0), self.unit(1, 1)
            self.right.wait_recv()
            self.on_right = copy(first, first, self.ring(1), self.group)
            self.on_right.start()
            self.left.wait_recv()
            self.on_left = copy(second, second, self.ring(SIDE - 1), self.group)
            self.on_left.start()

        def finish(self):
            self.on_right.wait_recv()
            self.on_left.wait_recv()

    class Gather:
        def __init__(self, start, count, group, x_first):
            along_x = lambda i, at: x_all.at[my, i, at]
            along_y = lambda i, at: x_all.at[i, mx, at]
            whole_y = lambda i, at: x_all.at[i, :, at]
            whole_x = lambda i, at: x_all.at[:, i, at]
            if x_first:
                self.one = Ring(along_x, mx, x_ring, start, count, group)
                self.two = Ring(whole_y, my, y_ring, start, count, group)
            else:
                self.one = Ring(along_y, my, y_ring, start, count, group)
                self.two = Ring(whole_x, mx, x_ring, start, count, group)

    class Rows:
        def __init__(self, start, count, group):
            self.gathers = Gather(start, count // 2, group, True), Gather(start + count // 2, count // 2, group, False)

        def arrive(self):
            pass

        def gather(self, phase, step):
            for g in self.gathers:
                getattr((g.one, g.two)[phase], step)()


    loads["xm"].wait()
    row_norm(xm, mix_gain_ref, mm)
    loads["pin"].wait()
    narrow = pin.shape[0]
    pooled_in = lax.dot_general(mm[...], pin[...], (((1,), (1,)), ((), ())), preferred_element_type=F32)
    pooled_in = jnp.concatenate([pooled_in, jnp.zeros((tok, LANES - narrow), F32)], axis=1).astype(BF16)
    halo_out[...] = pooled_in[tok - 16:, :]
    halo = copy(halo_out, halo_in, {"ep": (ep + 1) % n_ep, "tp": tp}, len(send_all) - 1)
    halo.start()

    loads["sg"].wait()
    loads["su"].wait()
    both = dot(mn[...], sgu[...])
    shared_rows = slice(rows_all, rows_all + tok)
    x_all[my, mx, shared_rows, :] = silu_mul(both[:, :LANES], both[:, LANES:]).astype(BF16)

    def windows():
        halo.wait_recv()
        carried = jnp.where(ep > 0, halo_in[...].astype(F32), 0.0)
        ext = jnp.concatenate([carried, pooled_in.astype(F32)], axis=0)
        sums, chosen, window = ext, None, 1
        for index in range(4):
            sums = sums + pltpu.roll(sums, window, 0)
            window *= 2
            chosen = sums if chosen is None else jnp.where(my >= index, sums, chosen)
        position = (ep * tok + lax.broadcasted_iota(jnp.int32, (tok, LANES), 0) + 1).astype(F32)
        widest = lax.shift_left(2, my).astype(F32)
        zeros_right = jnp.zeros((1, LANES - narrow), F32)
        pscale = jnp.concatenate([pscale_ref[...], zeros_right], axis=1)
        pgain = jnp.concatenate([pgain_ref[...], zeros_right], axis=1)
        scaled = (chosen[16:, :] / jnp.minimum(position, widest) - pooled_in.astype(F32)) * pscale
        squares = jnp.sum(scaled * scaled, axis=1, keepdims=True)
        squares = jnp.broadcast_to(squares, (tok, LANES)).T[0:8, :]
        sq_out[...] = squares

        @pl.loop(1, n_tp)
        def _(i):
            pltpu.make_async_remote_copy(
                src_ref=sq_out, dst_ref=sq_in.at[i - 1], send_sem=sq_send, recv_sem=sq_recv,
                device_id={"ep": ep, "tp": (tp + i) % n_tp}, device_id_type=MESH,
            ).start()
        return scaled, squares, pgain

    def combine_terms():
        high = weight.astype(BF16).astype(F32)
        low = weight - high
        for i in range(n_ep):
            at = slice(i * cap, (i + 1) * cap)
            same = place[i:i + 1, :] == slot_row
            chi[at, :] = jnp.where(same, high[i:i + 1, :], 0.0).astype(BF16)
            clo[at, :] = jnp.where(same, low[i:i + 1, :], 0.0).astype(BF16)

    pool_start = rows_all + tok

    def pool_norm(scaled, squares, pgain):
        pltpu.make_async_copy(sq_in, sq_in, sq_recv).wait()
        total = squares
        for i in range(n_tp - 1):
            total = total + sq_in[i]
        total = jnp.broadcast_to(total[0:1, :], (tok, LANES)).T
        pooled = (scaled * lax.rsqrt(total / (narrow * n_tp) + EPS) * pgain).astype(BF16).astype(F32)
        packed = pooled[:tok // 2, :] + pltpu.roll(pooled[tok // 2:, :], narrow, 1)
        x_all[my, mx, pool_start:pool_start + tok // 2, :] = packed.astype(BF16)

    count = rows_all // (2 * n_pairs)
    half = count // 2

    class RingSum:
        def __init__(self, view, me, ring, opp, main, start, group):
            self.view, self.me, self.ring, self.opp, self.main, self.start_row = view, me, ring, opp, main, start
            self.group = group

        def unit(self, step, part):
            lo, n = {None: (0, count), 0: (0, half), 1: (half, half)}[part]
            return self.view((self.me + step) % SIDE, pl.ds(self.start_row + lo, n))

        def into(self, side, part):
            at = pl.ds(part * half, half)
            return self.main.at[(side,) + (slice(None),) * (len(self.main.shape) - 3) + (at,)]

        def start(self):
            self.opp_right = copy(self.unit(2, 0), self.opp.at[0], self.ring(1), self.group)
            self.opp_left = copy(self.unit(2, 1), self.opp.at[1], self.ring(SIDE - 1), self.group)
            self.far_right = copy(self.unit(1, 1), self.into(0, 1), self.ring(1), self.group)
            self.far_left = copy(self.unit(SIDE - 1, 0), self.into(1, 0), self.ring(SIDE - 1), self.group)
            for made in (self.opp_right, self.opp_left, self.far_right, self.far_left):
                made.start()

        def add(self, unit, extra):
            unit[...] = (unit[...].astype(F32) + extra[...].astype(F32)).astype(BF16)

        def relay(self):
            self.opp_right.wait_recv()
            self.add(self.unit(1, 0), self.opp.at[0])
            self.near_right = copy(self.unit(1, 0), self.into(0, 0), self.ring(1), self.group)
            self.near_right.start()
            self.opp_left.wait_recv()
            self.add(self.unit(SIDE - 1, 1), self.opp.at[1])
            self.near_left = copy(self.unit(SIDE - 1, 1), self.into(1, 1), self.ring(SIDE - 1), self.group)
            self.near_left.start()

        def finish(self, dst):
            for made in (self.far_right, self.far_left, self.near_right, self.near_left):
                made.wait_recv()
            own = self.unit(0, None)
            dst[...] = (own[...].astype(F32) + self.main[0].astype(F32) + self.main[1].astype(F32)).astype(BF16)

    tile = min(256, count)

    def experts(start, rows):
        @pl.loop(0, rows // tile)
        def _(b):
            at = pl.ds(pl.multiple_of(start + b * tile, tile), tile)
            lhs = jnp.concatenate([x_all[i // SIDE, i % SIDE, at, :] for i in range(n_tp)], axis=1)
            pair = dot(lhs, wgu[...])
            hidden = silu_mul(pair[:, :LANES], pair[:, LANES:]).astype(BF16)
            for j in range(n_tp // 2):
                out = dot(hidden, wd[:, j * 2 * LANES:(j + 1) * 2 * LANES])
                for s in range(2):
                    i = 2 * j + s
                    part[i // SIDE, i % SIDE, at, :] = out[:, s * LANES:(s + 1) * LANES].astype(BF16)

    class Pair(Rows):
        def __init__(self, k):
            self.k = k
            self.a_start, self.b_start = 2 * k * count, (2 * k + 1) * count
            super().__init__(self.a_start, 2 * count, k)
            one = (
                RingSum(lambda i, at: part.at[i, :, at], my, y_ring, opp1.at[0, k], main1.at[0, k], self.a_start, k),
                RingSum(lambda i, at: part.at[:, i, at], mx, x_ring, opp1.at[1, k], main1.at[1, k], self.b_start, k),
            )
            two = (
                RingSum(lambda i, at: q_a.at[k, i, at], mx, x_ring, opp2.at[0, k], main2.at[0, k], 0, k),
                RingSum(lambda i, at: q_b.at[k, i, at], my, y_ring, opp2.at[1, k], main2.at[1, k], 0, k),
            )
            self.sums = (one, two)

        def arrive(self):
            lo = max(cap, self.a_start)
            got = x_all.at[my, mx, pl.ds(lo, self.a_start + 2 * count - lo)]
            pltpu.make_async_copy(got, got, z_recv.at[self.k]).wait()

        def compute(self):
            if self is pairs[0]:
                for name in ("eg", "eu", "ed"):
                    loads[name].wait()
            experts(self.a_start, 2 * count)

        def sum(self, phase, step):
            for s in self.sums[phase]:
                getattr(s, step)()

        def middle(self):
            self.sums[0][0].finish(q_a.at[self.k])
            self.sums[0][1].finish(q_b.at[self.k])

        def close(self):
            self.sums[1][0].finish(y_own.at[pl.ds(self.a_start, count)])
            self.sums[1][1].finish(y_own.at[pl.ds(self.b_start, count)])
            first = self.a_start // cap
            if first == 0:
                back[0:cap, :] = y_own[0:cap, :]

            @pl.loop(max(first, 1), first + 2 * count // cap)
            def _(i):
                at = pl.ds(pl.multiple_of(i * cap, cap), cap)
                pltpu.make_async_remote_copy(
                    src_ref=y_own.at[at], dst_ref=back.at[at], send_sem=zb_send, recv_sem=zb_recv.at[self.k],
                    device_id={"ep": peer_from(i), "tp": tp}, device_id_type=MESH,
                ).start()

    pairs = [Pair(k) for k in order]

    def plain_outputs():
        items[0].gather(1, "finish")
        items[-1].gather(1, "finish")
        for name in ("po_a", "po_b", "sd"):
            loads[name].wait()
        lane = lax.broadcasted_iota(jnp.int32, (tok // 2, LANES), 1)
        zero = jnp.zeros((tok // 2, LANES), BF16)
        upper, lower = [], []
        for i in range(n_tp):
            block = x_all[i // SIDE, i % SIDE, pool_start:pool_start + tok // 2, :]
            upper.append(jnp.where(lane < narrow, block, zero))
            lower.append(jnp.where(lane < narrow, zero, block))
        lhs = jnp.concatenate([jnp.concatenate(upper, axis=1), jnp.concatenate(lower, axis=1)], axis=0)
        mix_out_ref[...] = dot(lhs, po2[...].reshape(2 * n_tp * narrow, LANES)).astype(BF16)
        lhs = jnp.concatenate([x_all[i // SIDE, i % SIDE, shared_rows, :] for i in range(n_tp)], axis=1)
        result = dot(lhs, sd[...])
        return result

    items = [Rows(rows_all, tok, n_pairs)] + pairs + [Rows(pool_start, tok // 2, n_pairs + 1)]

    def gathered(index):
        return items[index] if 0 <= index < len(items) else None

    def summed(index):
        return pairs[index - 1] if 1 <= index <= n_pairs else None

    for s in range(n_pairs + 9):
        if s == 5:
            pool_norm(*pool_state)
        if p := gathered(s):
            p.arrive()
            p.gather(0, "start")
        if p := gathered(s - 1):
            p.gather(0, "relay")
        if p := gathered(s - 2):
            p.gather(0, "finish")
            p.gather(1, "start")
        if p := gathered(s - 3):
            p.gather(1, "relay")
        if p := summed(s - 4):
            p.gather(1, "finish")
            p.compute()
            p.sum(0, "start")
        if s == 1:
            pool_state = windows()
        if s == 2:
            combine_terms()
        if p := summed(s - 5):
            p.sum(0, "relay")
        if p := summed(s - 6):
            p.middle()
            p.sum(1, "start")
        if s == n_pairs + 6:
            result = plain_outputs()
        if p := summed(s - 7):
            p.sum(1, "relay")
        if p := summed(s - 8):
            p.close()

    over = (((0,), (0,)), ((), ()))
    for p in pairs:
        lo = max(cap, p.a_start)
        arrived = back.at[pl.ds(lo, p.a_start + 2 * count - lo)]
        pltpu.make_async_copy(arrived, arrived, zb_recv.at[p.k]).wait()
        at = slice(p.a_start, p.a_start + 2 * count)
        result += lax.dot_general(chi[at, :], back[at, :], over, preferred_element_type=F32)
        result += lax.dot_general(clo[at, :], back[at, :], over, preferred_element_type=F32)
    moe_out_ref[...] = result.astype(BF16)

    for group, size in enumerate(send_all):
        blocks = size // (60 * 16 * LANES)
        gone = halo_out if blocks == 0 else part.at[0, 0:blocks, 0:60 * 16]
        pltpu.make_async_copy(gone, gone, send_sems.at[group]).wait()
    for whole, sem in ((outgoing, z_send), (y_own, zb_send)):
        gone = whole.at[pl.ds(cap, rows_all - cap)]
        pltpu.make_async_copy(gone, gone, sem).wait()
    pltpu.make_async_copy(sq_in, sq_in, sq_send).wait()


def on_device(n_pairs, mix_input, expert_input, mix_gain, moe_gain, pool_in, pool_scale, pool_gain, pool_out, route,
              route_score, expert_gate, expert_up, expert_down, shared_gate, shared_up, shared_down):
    n_ep, n_tp = lax.axis_size("ep"), lax.axis_size("tp")
    tok, width = mix_input.shape
    top = route.shape[1]
    cap = 2 * tok * top // n_ep
    rows = cap * n_ep
    narrow = pool_in.shape[1]
    count = rows // (2 * n_pairs)
    everything = rows + tok + tok // 2
    vmem = pl.BlockSpec(memory_space=pltpu.VMEM)
    hbm = pl.BlockSpec(memory_space=pltpu.HBM)
    dma = pltpu.SemaphoreType.DMA
    n_copies = 1 + 32 + n_pairs * 40
    return pl.pallas_call(
        functools.partial(kernel, n_pairs),
        out_shape=(
            jax.ShapeDtypeStruct((tok, pool_out.shape[1]), BF16),
            jax.ShapeDtypeStruct((tok, shared_down.shape[1]), BF16),
        ),
        in_specs=[hbm, hbm, vmem, vmem, hbm, vmem, vmem, hbm, vmem, vmem, hbm, hbm, hbm, hbm, hbm, hbm],
        out_specs=(vmem, vmem),
        scratch_shapes=[
            pltpu.VMEM((tok, width), BF16),
            pltpu.VMEM((tok, width), BF16),
            pltpu.VMEM((width, 2 * LANES), BF16),
            pltpu.VMEM((LANES, width), BF16),
            pltpu.VMEM((width, 2 * LANES), BF16),
            pltpu.VMEM((width, LANES), BF16),
            pltpu.VMEM((narrow, width), BF16),
            pltpu.VMEM((n_tp, 2, narrow, LANES), BF16),
            pltpu.VMEM((tok, width), BF16),
            pltpu.VMEM((tok, width), BF16),
            pltpu.VMEM((rows, LANES), BF16),
            pltpu.VMEM((rows, LANES), BF16),
            pltpu.VMEM((rows, LANES), BF16),
            pltpu.VMEM((rows, LANES), BF16),
            pltpu.VMEM((SIDE, SIDE, everything, LANES), BF16),
            pltpu.VMEM((SIDE, SIDE, rows, LANES), BF16),
            pltpu.VMEM((n_pairs, SIDE, count, LANES), BF16),
            pltpu.VMEM((n_pairs, SIDE, count, LANES), BF16),
            pltpu.VMEM((rows, LANES), BF16),
            pltpu.VMEM((rows, LANES), BF16),
            pltpu.VMEM((2, n_pairs, 2, SIDE, count // 2, LANES), BF16),
            pltpu.VMEM((2, n_pairs, 2, SIDE, count, LANES), BF16),
            pltpu.VMEM((2, n_pairs, 2, count // 2, LANES), BF16),
            pltpu.VMEM((2, n_pairs, 2, count, LANES), BF16),
            pltpu.VMEM((16, LANES), BF16),
            pltpu.VMEM((16, LANES), BF16),
            pltpu.VMEM((8, LANES), F32),
            pltpu.VMEM((n_tp - 1, 8, LANES), F32),
            dma((11,)),
            dma((n_pairs + 3,)),
            dma((n_copies,)),
            dma,
            dma((n_pairs,)),
            dma,
            dma((n_pairs,)),
            dma,
            dma,
        ],
        compiler_params=pltpu.CompilerParams(
            collective_id=0, has_side_effects=True, vmem_limit_bytes=60 * 1024 * 1024
        ),
    )(
        expert_input,
        mix_input,
        mix_gain.reshape(1, -1),
        moe_gain.reshape(1, -1),
        pool_in.T,
        pool_scale.reshape(1, -1),
        pool_gain.reshape(1, -1),
        pool_out.reshape(n_tp, narrow, pool_out.shape[1]),
        route.T,
        route_score.T,
        expert_gate,
        expert_up,
        expert_down,
        shared_gate,
        shared_up,
        shared_down,
    )


def solution(mesh):
    return jax.shard_map(
        functools.partial(on_device, 8),
        mesh=mesh,
        in_specs=(
            P("ep", None),
            P("ep", None),
            P(),
            P(),
            P(None, "tp"),
            P("tp"),
            P("tp"),
            P(None, "tp"),
            P("ep", None),
            P("ep", None),
            P("ep", None, "tp"),
            P("ep", None, "tp"),
            P("ep", "tp", None),
            P(None, "tp"),
            P(None, "tp"),
            P(None, "tp"),
        ),
        out_specs=(P("ep", "tp"), P("ep", "tp")),
        check_vma=False,
    )
```

time: 129 us -> 98.5 us (0.76)
  Pallas kernels: 122 us -> 95.6 us
  local copies, waits for them, and re-layouts: 6.08 us -> 2 us
    pallas_call x1, Pallas kernels: 122 us -> 95.6 us  [on_device(): pl.pallas_call(functools.partial(kernel, n_pairs), out_shape=(jax.ShapeDt...]
    unnamed x11 -> x4, local copies, waits for them, and re-layouts: 6.08 us -> 2 us
where the time goes in v2:
time: 98.5 us; the launch traced here: 98.3 us
  Pallas kernels  95.6 us (97%)
  local copies, waits for them, and re-layouts  2 us (2%)
    pallas_call x1, Pallas kernels, on_device(): pl.pallas_call(functools.partial(kernel, n_pairs), out_shape=(jax.ShapeDt...  95.6 us
    unnamed x4, local copies, waits for them, and re-layouts  2 us

profile of v2, /device:TPU:1, one launch (start us, length us, event | category | flops | bytes accessed | tf_op | source)
XLA Modules:
  0.0 98.3 jit_solution(5231993427392073206)
XLA Ops:
  0.6 95.6 %shard_map.167 = (bf16[128,128]{1,0:T(8,128)(2,1)}, bf16[128,128]{1,0:T(8,128)(2,1)}) custom-call(bf16[128,2048]{1,0:T(8,128)(2,1)} %xe_hbm.1, bf16[128,2048]{1,0:T(8,128)(2,1)} %xm_hbm.1, f32[1,2048]{1,0:T(1,128)} %bitcast.10, f32[1,2048]{1,0:T(1,128)} %bitcast.11, bf16[64,2048]{1,0:T(8,128)(2,1)} %bitcast.8, f32[1,64]{1,0:T(1,128)} %bitcast.14, ...), custom_call_target="tpu_custom_call" | custom-call | tf_op jit(solution)/shard_map/pallas_call | solution.py:486
  96.3 0.0 copy-start
  96.3 1.4 %copy.20 = bf16[128,128]{1,0:T(8,128)(2,1)} copy(bf16[128,128]{1,0:T(8,128)(2,1)} %get-tuple-element.4) | data formatting | bytes 65536
  97.7 0.0 copy-done
  97.7 0.6 copy.21
Async XLA Ops:
  96.3 1.4 %copy-start = (bf16[128,128]{1,0:T(8,128)(2,1)S(1)}, bf16[128,128]{1,0:T(8,128)(2,1)}, u32[]{:S(2)}) copy-start(bf16[128,128]{1,0:T(8,128)(2,1)} %get-tuple-element.5) | copy-start | bytes 98308

commit v3 on v2

v3 whole, which is shorter than its diff:
```python
import functools

import jax
import jax.numpy as jnp
from jax import lax
from jax.experimental import pallas as pl
from jax.experimental.pallas import tpu as pltpu
from jax.sharding import PartitionSpec as P

MESH = pl.DeviceIdType.MESH
F32, BF16 = jnp.float32, jnp.bfloat16
EPS = 1e-06
SIDE = 4
DISPATCH_TICK, WINDOW_TICK, POOL_TICK = 1, 8, 14
LAGS = {"relay": 2, "along": 4, "along_relay": 6, "compute": 8, "first_relay": 10, "second": 12, "second_relay": 14, "close": 16}
LANES = 128


def dot(a, b):
    return jnp.dot(a, b, preferred_element_type=F32)


def silu_mul(gate, upper):
    return gate / (1.0 + jnp.exp(-gate)) * upper


def kernel(
    n_pairs,
    xe_hbm, xm_hbm, mix_gain_ref, moe_gain_ref, pin_hbm, pscale_ref, pgain_ref, pout_hbm, route_ref, score_ref,
    eg_hbm, eu_hbm, ed_hbm, sg_hbm, su_hbm, sd_hbm,
    out_ref,
    xe, xm, wgu, wd, sgu, sd, pin, po2, mn, mm, sel, chi, clo, outgoing, x_all, part, q_a, q_b, y_own, back,
    opp1, main1, opp2, main2, halo_out, halo_in, sq_out, sq_in,
    load_sems, send_sems, recv_sems, rows_sems, z_send, z_recv, zb_send, zb_recv, sq_send, sq_recv,
):
    n_ep, n_tp = lax.axis_size("ep"), lax.axis_size("tp")
    ep, tp = lax.axis_index("ep"), lax.axis_index("tp")
    n_z = n_ep // 2
    z, core = ep // 2, ep % 2
    my, mx = tp // SIDE, tp % SIDE
    tok, width = xe_hbm.shape
    rows_all = outgoing.shape[0]
    cap = rows_all // n_ep

    def wrap(value, size):
        return lax.rem(value, size)

    z_bits = [wrap(z // 2 ** b, 2) for b in range(8) if 2 ** b < n_z]
    late = z // (n_z // 2)

    def peer(i):
        other = z
        for b, bit in enumerate(z_bits):
            if i // 2 // 2 ** b % 2:
                other = other + 2 ** b * (1 - 2 * bit)
        return other * 2 + wrap(core + i % 2, 2)

    def by_half(low, high):
        return low if isinstance(low, int) and low == high else low + late * (high - low)

    loads = {}

    def load(name, src, dst):
        loads[name] = pltpu.make_async_copy(src, dst, load_sems.at[len(loads)])
        loads[name].start()

    load("xe", xe_hbm, xe)

    barrier = pltpu.get_barrier_semaphore()
    for i in range(n_ep - 1, 0, -1):
        pl.semaphore_signal(barrier, inc=1, device_id={"ep": peer(i), "tp": tp}, device_id_type=MESH)
    for i in range(1, n_tp):
        pl.semaphore_signal(barrier, inc=1, device_id={"ep": ep, "tp": wrap(tp + i, n_tp)}, device_id_type=MESH)

    load("xm", xm_hbm, xm)
    load("pin", pin_hbm, pin)
    load("sg", sg_hbm, sgu.at[:, 0:LANES])
    load("su", su_hbm, sgu.at[:, LANES:2 * LANES])
    load("eg", eg_hbm.at[0], wgu.at[:, 0:LANES])
    load("eu", eu_hbm.at[0], wgu.at[:, LANES:2 * LANES])
    load("ed", ed_hbm.at[0], wd)
    load("po_a", pout_hbm, po2.at[:, 0])
    load("po_b", pout_hbm, po2.at[:, 1])
    load("sd", sd_hbm, sd)

    def row_norm(src, gain_ref, dst):
        for b in range(tok // 16):
            at = slice(b * 16, (b + 1) * 16)
            values = src[at, :].astype(F32)
            scale = lax.rsqrt(jnp.mean(values * values, axis=-1, keepdims=True) + EPS)
            dst[at, :] = (values * scale * gain_ref[...]).astype(BF16)


    top = route_ref.shape[0]
    routes = [route_ref[k:k + 1, :].astype(F32) for k in range(top)]
    scores = [score_ref[k:k + 1, :] for k in range(top)]
    slot_i = lax.broadcasted_iota(jnp.int32, (n_ep, tok), 0)
    expert_i = (((slot_i // 2) ^ z) * 2 + ((slot_i % 2) ^ core)).astype(F32)
    total = scores[0]
    for k in range(1, top):
        total = total + scores[k]
    hit = jnp.zeros((n_ep, tok), F32)
    weight = jnp.zeros((n_ep, tok), F32)
    for k in range(top):
        same = expert_i == routes[k]
        hit = jnp.where(same, 1.0, hit)
        weight = jnp.where(same, 2.5 * scores[k] / total, weight)
    before = (
        lax.broadcasted_iota(jnp.int32, (tok, tok), 0) < lax.broadcasted_iota(jnp.int32, (tok, tok), 1)
    )
    rank = dot(hit.astype(BF16), jnp.where(before, 1.0, 0.0).astype(BF16))
    place = jnp.where(hit > 0.0, rank, -1.0)
    slot_row = lax.broadcasted_iota(jnp.int32, (cap, tok), 0).astype(F32)
    for i in range(n_ep):
        sel[i * cap:(i + 1) * cap, :] = jnp.where(place[i:i + 1, :] == slot_row, 1.0, 0.0).astype(BF16)

    loads["xe"].wait()
    row_norm(xe, moe_gain_ref, mn)
    share = mn[:, pl.ds(pl.multiple_of(tp * LANES, LANES), LANES)]
    outgoing[...] = dot(sel[...], share).astype(BF16)
    x_all[my, mx, 0:cap, :] = outgoing[0:cap, :]

    loads["sg"].wait()
    loads["su"].wait()
    both = dot(mn[...], sgu[...])
    shared_rows = slice(rows_all, rows_all + tok)
    x_all[my, mx, shared_rows, :] = silu_mul(both[:, :LANES], both[:, LANES:]).astype(BF16)

    pl.semaphore_wait(barrier, n_ep - 1 + n_tp - 1)

    middle, quarter = n_pairs // 2, n_pairs // 4
    low_order = list(range(n_pairs - 2)) + [n_pairs - 1, n_pairs - 2]
    high_order = list(range(quarter)) + list(range(middle, n_pairs)) + list(range(middle - 1, quarter - 1, -1))
    per_pair = n_ep // n_pairs

    def dispatch(chunks):
        for i in [i for k in chunks for i in range(max(1, k * per_pair), (k + 1) * per_pair)]:
            at = pl.ds(i * cap, cap)
            pltpu.make_async_remote_copy(
                src_ref=outgoing.at[at], dst_ref=x_all.at[my, mx, at], send_sem=z_send,
                recv_sem=z_recv.at[i // per_pair], device_id={"ep": peer(i), "tp": tp}, device_id_type=MESH,
            ).start()

    dispatch(range(quarter))

    x_ring = lambda step: {"ep": ep, "tp": my * SIDE + wrap(mx + step, SIDE)}
    y_ring = lambda step: {"ep": ep, "tp": wrap(my + step, SIDE) * SIDE + mx}

    def send_of(group):
        return send_sems.at[group // quarter if group < n_pairs else 4 + group - n_pairs]

    def recv_of(group, stage):
        return recv_sems.at[group, stage] if group < n_pairs else rows_sems.at[group - n_pairs, stage]

    def launch(group, stage, src, dst, where):
        pltpu.make_async_remote_copy(
            src_ref=src, dst_ref=dst, send_sem=send_of(group), recv_sem=recv_of(group, stage),
            device_id=where, device_id_type=MESH,
        ).start()

    def await_rows(sem, units, rows):
        spot = {2: part.at[0, 0:2, 0:rows], 4: part.at[0, :, 0:rows], 8: part.at[0:2, :, 0:rows],
                16: part.at[:, :, 0:rows]}[units]
        pltpu.make_async_copy(spot, spot, sem).wait()

    class Ring:
        def __init__(self, view, me, ring, start, count):
            self.view, self.me, self.ring, self.start_row, self.count = view, me, ring, start, count

        def unit(self, step, half=None):
            lo, n = (0, self.count) if half is None else (half * self.count // 2, self.count // 2)
            return self.view(wrap(self.me + step, SIDE), pl.ds(self.start_row + lo, n))

        def own(self, group, stage):
            unit = self.unit(0)
            launch(group, stage, unit, unit, self.ring(1))
            launch(group, stage, unit, unit, self.ring(SIDE - 1))

        def onward(self, group, stage):
            first, second = self.unit(SIDE - 1, 0), self.unit(1, 1)
            launch(group, stage, first, first, self.ring(1))
            launch(group, stage, second, second, self.ring(SIDE - 1))

    class Rows:
        def __init__(self, start, rows, group):
            self.group, self.count = group, rows // 2
            a, b = (start, self.count), (start + self.count, self.count)
            self.rings = (
                (
                    Ring(lambda i, at: x_all.at[my, i, at], mx, x_ring, *a),
                    Ring(lambda i, at: x_all.at[i, mx, at], my, y_ring, *b),
                ),
                (
                    Ring(lambda i, at: x_all.at[i, :, at], my, y_ring, *a),
                    Ring(lambda i, at: x_all.at[:, i, at], mx, x_ring, *b),
                ),
            )

        def arrive(self):
            pass

        def gather_start(self, phase):
            for ring in self.rings[phase]:
                ring.own(self.group, 2 * phase)

        def gather_relay(self, phase):
            await_rows(recv_of(self.group, 2 * phase), (4, 16)[phase], self.count)
            for ring in self.rings[phase]:
                ring.onward(self.group, 2 * phase + 1)

        def gather_finish(self, phase):
            await_rows(recv_of(self.group, 2 * phase + 1), (2, 8)[phase], self.count)

    narrow = pin.shape[0]

    def mix_local():
        loads["xm"].wait()
        row_norm(xm, mix_gain_ref, mm)
        loads["pin"].wait()
        pooled_in = lax.dot_general(mm[...], pin[...], (((1,), (1,)), ((), ())), preferred_element_type=F32)
        pooled_in = jnp.concatenate([pooled_in, jnp.zeros((tok, LANES - narrow), F32)], axis=1).astype(BF16)
        halo_out[...] = pooled_in[tok - 16:, :]
        halo = pltpu.make_async_remote_copy(
            src_ref=halo_out, dst_ref=halo_in, send_sem=sq_send.at[1], recv_sem=sq_recv.at[1],
            device_id={"ep": wrap(ep + 1, n_ep), "tp": tp}, device_id_type=MESH,
        )
        halo.start()
        return pooled_in, halo

    def windows(pooled_in, halo):
        halo.wait_recv()
        carried = jnp.where(ep > 0, halo_in[...].astype(F32), 0.0)
        ext = jnp.concatenate([carried, pooled_in.astype(F32)], axis=0)
        sums, chosen, window = ext, None, 1
        for index in range(4):
            sums = sums + pltpu.roll(sums, window, 0)
            window *= 2
            chosen = sums if chosen is None else jnp.where(my >= index, sums, chosen)
        position = (ep * tok + lax.broadcasted_iota(jnp.int32, (tok, LANES), 0) + 1).astype(F32)
        widest = lax.shift_left(2, my).astype(F32)
        zeros_right = jnp.zeros((1, LANES - narrow), F32)
        pscale = jnp.concatenate([pscale_ref[...], zeros_right], axis=1)
        pgain = jnp.concatenate([pgain_ref[...], zeros_right], axis=1)
        scaled = (chosen[16:, :] / jnp.minimum(position, widest) - pooled_in.astype(F32)) * pscale
        squares = jnp.sum(scaled * scaled, axis=1, keepdims=True)
        squares = jnp.broadcast_to(squares, (tok, LANES)).T[0:8, :]
        sq_out[...] = squares

        for i in range(1, n_tp):
            pltpu.make_async_remote_copy(
                src_ref=sq_out, dst_ref=sq_in.at[i - 1], send_sem=sq_send.at[0], recv_sem=sq_recv.at[0],
                device_id={"ep": ep, "tp": wrap(tp + i, n_tp)}, device_id_type=MESH,
            ).start()
        return scaled, squares, pgain

    def combine_terms():
        high = weight.astype(BF16).astype(F32)
        low = weight - high
        for i in range(n_ep):
            at = slice(i * cap, (i + 1) * cap)
            same = place[i:i + 1, :] == slot_row
            chi[at, :] = jnp.where(same, high[i:i + 1, :], 0.0).astype(BF16)
            clo[at, :] = jnp.where(same, low[i:i + 1, :], 0.0).astype(BF16)

    pool_start = rows_all + tok

    def pool_norm(scaled, squares, pgain):
        pltpu.make_async_copy(sq_in, sq_in, sq_recv.at[0]).wait()
        total = squares
        for i in range(n_tp - 1):
            total = total + sq_in[i]
        total = jnp.broadcast_to(total[0:1, :], (tok, LANES)).T
        pooled = (scaled * lax.rsqrt(total / (narrow * n_tp) + EPS) * pgain).astype(BF16).astype(F32)
        packed = pooled[:tok // 2, :] + pltpu.roll(pooled[tok // 2:, :], narrow, 1)
        x_all[my, mx, pool_start:pool_start + tok // 2, :] = packed.astype(BF16)

    count = rows_all // (2 * n_pairs)
    half = count // 2

    class RingSum:
        def __init__(self, view, me, ring, opp, main, start):
            self.view, self.me, self.ring, self.opp, self.main, self.start_row = view, me, ring, opp, main, start

        def unit(self, step, which=None):
            lo, n = (0, count) if which is None else (which * half, half)
            return self.view(wrap(self.me + step, SIDE), pl.ds(self.start_row + lo, n))

        def into(self, side, which):
            at = pl.ds(which * half, half)
            return self.main.at[(side,) + (slice(None),) * (len(self.main.shape) - 3) + (at,)]

        def across(self, group, stage):
            launch(group, stage, self.unit(2, 0), self.opp.at[0], self.ring(1))
            launch(group, stage, self.unit(2, 1), self.opp.at[1], self.ring(SIDE - 1))

        def plain(self, group, stage):
            launch(group, stage, self.unit(1, 1), self.into(0, 1), self.ring(1))
            launch(group, stage, self.unit(SIDE - 1, 0), self.into(1, 0), self.ring(SIDE - 1))

        def added(self, group, stage):
            for unit, extra, dst, where in (
                (self.unit(1, 0), self.opp.at[0], self.into(0, 0), self.ring(1)),
                (self.unit(SIDE - 1, 1), self.opp.at[1], self.into(1, 1), self.ring(SIDE - 1)),
            ):
                unit[...] = (unit[...].astype(F32) + extra[...].astype(F32)).astype(BF16)
                launch(group, stage, unit, dst, where)

        def total(self, dst):
            own = self.unit(0)
            dst[...] = (own[...].astype(F32) + self.main[0].astype(F32) + self.main[1].astype(F32)).astype(BF16)

    tile = min(256, 2 * count)

    def experts(start, rows):
        @pl.loop(0, rows // tile)
        def _(b):
            at = pl.ds(pl.multiple_of(start + b * tile, tile), tile)
            lhs = jnp.concatenate([x_all[i // SIDE, i % SIDE, at, :] for i in range(n_tp)], axis=1)
            pair = dot(lhs, wgu[...])
            hidden = silu_mul(pair[:, :LANES], pair[:, LANES:]).astype(BF16)
            for j in range(n_tp // 2):
                out = dot(hidden, wd[:, j * 2 * LANES:(j + 1) * 2 * LANES])
                for s in range(2):
                    i = 2 * j + s
                    part[i // SIDE, i % SIDE, at, :] = out[:, s * LANES:(s + 1) * LANES].astype(BF16)

    class Pair(Rows):
        def __init__(self, k):
            self.k, self.chunks = k, (low_order[k], high_order[k])
            self.chunk = by_half(*self.chunks)
            self.start = self.chunk * (2 * count)
            if k > 0:
                self.start = pl.multiple_of(self.start, 2 * count)
            super().__init__(self.start, 2 * count, k)
            self.sums = (
                (
                    RingSum(lambda i, at: part.at[i, :, at], my, y_ring, opp1.at[0, k], main1.at[0, k], self.start),
                    RingSum(
                        lambda i, at: part.at[:, i, at], mx, x_ring, opp1.at[1, k], main1.at[1, k], self.start + count
                    ),
                ),
                (
                    RingSum(lambda i, at: q_a.at[k, i, at], mx, x_ring, opp2.at[0, k], main2.at[0, k], 0),
                    RingSum(lambda i, at: q_b.at[k, i, at], my, y_ring, opp2.at[1, k], main2.at[1, k], 0),
                ),
            )

        def arrive(self):
            lo = cap if self.k == 0 else 0
            got = x_all.at[my, mx, pl.ds(self.start + lo, 2 * count - lo)]
            pltpu.make_async_copy(got, got, z_recv.at[self.chunk]).wait()

        def compute(self):
            if self is pairs[0]:
                for name in ("eg", "eu", "ed"):
                    loads[name].wait()
            experts(self.start, 2 * count)

        def sum_start(self, phase):
            for ring in self.sums[phase]:
                ring.across(self.group, 4 + 2 * phase)
            for ring in self.sums[phase]:
                ring.plain(self.group, 5 + 2 * phase)

        def sum_relay(self, phase):
            await_rows(recv_of(self.group, 4 + 2 * phase), (8, 2)[phase], count)
            for ring in self.sums[phase]:
                ring.added(self.group, 5 + 2 * phase)

        def sum_finish(self, phase):
            await_rows(recv_of(self.group, 5 + 2 * phase), (16, 4)[phase], count)
            if phase == 0:
                targets = q_a.at[self.k], q_b.at[self.k]
            else:
                targets = y_own.at[pl.ds(self.start, count)], y_own.at[pl.ds(self.start + count, count)]
            for ring, dst in zip(self.sums[phase], targets):
                ring.total(dst)

        def send_back(self):
            if self.k == 0:
                back[0:cap, :] = y_own[0:cap, :]
            for i in range(self.k == 0, per_pair):
                at = pl.ds(pl.multiple_of(self.start + i * cap, cap), cap)
                low, high = (peer(chunk * per_pair + i) for chunk in self.chunks)
                pltpu.make_async_remote_copy(
                    src_ref=y_own.at[at], dst_ref=back.at[at], send_sem=zb_send, recv_sem=zb_recv,
                    device_id={"ep": by_half(low, high), "tp": tp}, device_id_type=MESH,
                ).start()

    pairs = [Pair(k) for k in range(n_pairs)]

    def plain_outputs():
        items[0].gather_finish(1)
        items[-1].gather_finish(1)
        for name in ("po_a", "po_b", "sd"):
            loads[name].wait()
        lane = lax.broadcasted_iota(jnp.int32, (tok // 2, LANES), 1)
        zero = jnp.zeros((tok // 2, LANES), BF16)
        upper, lower = [], []
        for i in range(n_tp):
            block = x_all[i // SIDE, i % SIDE, pool_start:pool_start + tok // 2, :]
            upper.append(jnp.where(lane < narrow, block, zero))
            lower.append(jnp.where(lane < narrow, zero, block))
        lhs = jnp.concatenate([jnp.concatenate(upper, axis=1), jnp.concatenate(lower, axis=1)], axis=0)
        out_ref[0] = dot(lhs, po2[...].reshape(2 * n_tp * narrow, LANES)).astype(BF16)
        lhs = jnp.concatenate([x_all[i // SIDE, i % SIDE, shared_rows, :] for i in range(n_tp)], axis=1)
        result = dot(lhs, sd[...])
        return result

    items = [Rows(rows_all, tok, n_pairs)] + pairs + [Rows(pool_start, tok // 2, n_pairs + 1)]

    def gathered(index):
        return items[index] if 0 <= index < len(items) else None

    def summed(index):
        return pairs[index - 1] if 1 <= index <= n_pairs else None

    for s in range(n_pairs + 1 + LAGS["close"]):
        if s == POOL_TICK:
            pool_norm(*pool_state)
        if p := gathered(s - LAGS["along"]):
            p.gather_finish(0)
            p.gather_start(1)
        if p := gathered(s - LAGS["relay"]):
            p.gather_relay(0)
        if p := gathered(s - LAGS["along_relay"]):
            p.gather_relay(1)
        if p := gathered(s):
            p.arrive()
            p.gather_start(0)
        if s == DISPATCH_TICK:
            dispatch([k for j in range(quarter) for k in (middle + j, quarter + j)] + list(range(middle + quarter, n_pairs)))
        if s == 0:
            pooled_in, halo = mix_local()
        if s == 2:
            combine_terms()
        if s == WINDOW_TICK:
            pool_state = windows(pooled_in, halo)
        if p := summed(s - LAGS["close"]):
            p.sum_finish(1)
            p.send_back()
        if p := summed(s - LAGS["second_relay"]):
            p.sum_relay(1)
        if p := summed(s - LAGS["second"]):
            p.sum_finish(0)
            p.sum_start(1)
        if p := summed(s - LAGS["first_relay"]):
            p.sum_relay(0)
        if p := summed(s - LAGS["compute"]):
            p.gather_finish(1)
            p.compute()
            p.sum_start(0)
        if s == n_pairs - 1 + LAGS["close"]:
            result = plain_outputs()

    over = (((0,), (0,)), ((), ()))
    arrived = back.at[pl.ds(cap, rows_all - cap)]
    pltpu.make_async_copy(arrived, arrived, zb_recv).wait()
    result += lax.dot_general(chi[...], back[...], over, preferred_element_type=F32)
    result += lax.dot_general(clo[...], back[...], over, preferred_element_type=F32)
    out_ref[1] = result.astype(BF16)

    halo.wait_send()
    sent = [part.at[0:2, :, 0:30 * count]] * 4 + [part.at[0, 0:2, 0:15 * p.count] for p in (items[0], items[-1])]
    for at, gone in enumerate(sent):
        pltpu.make_async_copy(gone, gone, send_sems.at[at]).wait()
    for whole, sem in ((outgoing, z_send), (y_own, zb_send)):
        gone = whole.at[pl.ds(cap, rows_all - cap)]
        pltpu.make_async_copy(gone, gone, sem).wait()
    pltpu.make_async_copy(sq_in, sq_in, sq_send.at[0]).wait()


def on_device(n_pairs, mix_input, expert_input, mix_gain, moe_gain, pool_in, pool_scale, pool_gain, pool_out, route,
              route_score, expert_gate, expert_up, expert_down, shared_gate, shared_up, shared_down):
    n_ep, n_tp = lax.axis_size("ep"), lax.axis_size("tp")
    tok, width = mix_input.shape
    top = route.shape[1]
    cap = 2 * tok * top // n_ep
    rows = cap * n_ep
    narrow = pool_in.shape[1]
    count = rows // (2 * n_pairs)
    everything = rows + tok + tok // 2
    vmem = pl.BlockSpec(memory_space=pltpu.VMEM)
    hbm = pl.BlockSpec(memory_space=pltpu.HBM)
    dma = pltpu.SemaphoreType.DMA
    both = pl.pallas_call(
        functools.partial(kernel, n_pairs),
        out_shape=jax.ShapeDtypeStruct((2, tok, shared_down.shape[1]), BF16),
        in_specs=[hbm, hbm, vmem, vmem, hbm, vmem, vmem, hbm, vmem, vmem, hbm, hbm, hbm, hbm, hbm, hbm],
        out_specs=vmem,
        scratch_shapes=[
            pltpu.VMEM((tok, width), BF16),
            pltpu.VMEM((tok, width), BF16),
            pltpu.VMEM((width, 2 * LANES), BF16),
            pltpu.VMEM((LANES, width), BF16),
            pltpu.VMEM((width, 2 * LANES), BF16),
            pltpu.VMEM((width, LANES), BF16),
            pltpu.VMEM((narrow, width), BF16),
            pltpu.VMEM((n_tp, 2, narrow, LANES), BF16),
            pltpu.VMEM((tok, width), BF16),
            pltpu.VMEM((tok, width), BF16),
            pltpu.VMEM((rows, LANES), BF16),
            pltpu.VMEM((rows, LANES), BF16),
            pltpu.VMEM((rows, LANES), BF16),
            pltpu.VMEM((rows, LANES), BF16),
            pltpu.VMEM((SIDE, SIDE, everything, LANES), BF16),
            pltpu.VMEM((SIDE, SIDE, rows, LANES), BF16),
            pltpu.VMEM((n_pairs, SIDE, count, LANES), BF16),
            pltpu.VMEM((n_pairs, SIDE, count, LANES), BF16),
            pltpu.VMEM((rows, LANES), BF16),
            pltpu.VMEM((rows, LANES), BF16),
            pltpu.VMEM((2, n_pairs, 2, SIDE, count // 2, LANES), BF16),
            pltpu.VMEM((2, n_pairs, 2, SIDE, count, LANES), BF16),
            pltpu.VMEM((2, n_pairs, 2, count // 2, LANES), BF16),
            pltpu.VMEM((2, n_pairs, 2, count, LANES), BF16),
            pltpu.VMEM((16, LANES), BF16),
            pltpu.VMEM((16, LANES), BF16),
            pltpu.VMEM((8, LANES), F32),
            pltpu.VMEM((n_tp - 1, 8, LANES), F32),
            dma((11,)),
            dma((6,)),
            dma((n_pairs, 8)),
            dma((2, 4)),
            dma,
            dma((n_pairs,)),
            dma,
            dma,
            dma((2,)),
            dma((2,)),
        ],
        compiler_params=pltpu.CompilerParams(
            collective_id=0, has_side_effects=True, vmem_limit_bytes=60 * 1024 * 1024
        ),
    )(
        expert_input,
        mix_input,
        mix_gain.reshape(1, -1),
        moe_gain.reshape(1, -1),
        pool_in.T,
        pool_scale.reshape(1, -1),
        pool_gain.reshape(1, -1),
        pool_out.reshape(n_tp, narrow, pool_out.shape[1]),
        route.T,
        route_score.T,
        expert_gate,
        expert_up,
        expert_down,
        shared_gate,
        shared_up,
        shared_down,
    )
    return both[0], both[1]


def solution(mesh):
    return jax.shard_map(
        functools.partial(on_device, 16),
        mesh=mesh,
        in_specs=(
            P("ep", None),
            P("ep", None),
            P(),
            P(),
            P(None, "tp"),
            P("tp"),
            P("tp"),
            P(None, "tp"),
            P("ep", None),
            P("ep", None),
            P("ep", None, "tp"),
            P("ep", None, "tp"),
            P("ep", "tp", None),
            P(None, "tp"),
            P(None, "tp"),
            P(None, "tp"),
        ),
        out_specs=(P("ep", "tp"), P("ep", "tp")),
        check_vma=False,
    )
```

time: 98.5 us -> 90.2 us (0.916)
  the two profiles are of different devices: /device:TPU:1 before, /device:TPU:2 now
where the time goes in v3:
time: 90.2 us; the launch traced here: 89.9 us
  Pallas kernels  87.9 us (97%)
  local copies, waits for them, and re-layouts  1.4 us (2%)
    pallas_call x1, Pallas kernels, on_device(): pl.pallas_call(functools.partial(kernel, n_pairs), out_shape=jax.ShapeDty...  87.9 us

profile of v3, /device:TPU:2, one launch (start us, length us, event | category | flops | bytes accessed | tf_op | source)
XLA Modules:
  0.0 89.9 jit_solution(10082394228260137169)
XLA Ops:
  0.6 87.9 %shard_map.167 = bf16[2,128,128]{2,1,0:T(8,128)(2,1)} custom-call(bf16[128,2048]{1,0:T(8,128)(2,1)} %xe_hbm.1, bf16[128,2048]{1,0:T(8,128)(2,1)} %xm_hbm.1, f32[1,2048]{1,0:T(1,128)} %bitcast.14, f32[1,2048]{1,0:T(1,128)} %bitcast.15, bf16[64,2048]{1,0:T(8,128)(2,1)} %bitcast.12, f32[1,64]{1,0:T(1,128)} %bitcast.18, f32[1,64]{1,0:T(1,128)} %bitcast.19, ...), custom_call_target="tpu_custom_call" | custom-call | tf_op jit(solution)/shard_map/pallas_call | solution.py:486
  88.5 1.4 %slice_bitcast_fusion = (bf16[128,128]{1,0:T(8,128)(2,1)}, bf16[128,128]{1,0:T(8,128)(2,1)}) fusion(bf16[2,128,128]{2,1,0:T(8,128)(2,1)} %shard_map.167), kind=kLoop, calls=%fused_computation | loop fusion | bytes 131072 | tf_op jit(solution)/shard_map/squeeze | solution.py:552

commit v4 on v3

--- a/solution.py
+++ b/solution.py
@@ -11,7 +11,7 @@
 F32, BF16 = jnp.float32, jnp.bfloat16
 EPS = 1e-06
 SIDE = 4
-DISPATCH_TICK, WINDOW_TICK, POOL_TICK = 1, 8, 14
+DISPATCH_TICKS, WINDOW_TICK, POOL_TICK = (1, 3, 6), 8, 14
 LAGS = {"relay": 2, "along": 4, "along_relay": 6, "compute": 8, "first_relay": 10, "second": 12, "second_relay": 14, "close": 16}
 LANES = 128
 
@@ -130,7 +130,8 @@
 
     middle, quarter = n_pairs // 2, n_pairs // 4
     low_order = list(range(n_pairs - 2)) + [n_pairs - 1, n_pairs - 2]
-    high_order = list(range(quarter)) + list(range(middle, n_pairs)) + list(range(middle - 1, quarter - 1, -1))
+    third, fourth = list(range(middle, middle + quarter)), list(range(middle + quarter, n_pairs))
+    high_order = list(range(quarter)) + fourth + third + list(range(middle - 1, quarter - 1, -1))
     per_pair = n_ep // n_pairs
 
     def dispatch(chunks):
@@ -142,6 +143,19 @@
             ).start()
 
     dispatch(range(quarter))
+
+    def dispatch_later(turn):
+        second = list(range(quarter, middle))
+        low = ([k for pair in zip(fourth, second) for k in pair], third, [])[turn]
+        high = ([], third + fourth, second[::-1])[turn]
+
+        @pl.when(late == 0)
+        def _():
+            dispatch(low)
+
+        @pl.when(late == 1)
+        def _():
+            dispatch(high)
 
     x_ring = lambda step: {"ep": ep, "tp": my * SIDE + wrap(mx + step, SIDE)}
     y_ring = lambda step: {"ep": ep, "tp": wrap(my + step, SIDE) * SIDE + mx}
@@ -428,8 +442,8 @@
         if p := gathered(s):
             p.arrive()
             p.gather_start(0)
-        if s == DISPATCH_TICK:
-            dispatch([k for j in range(quarter) for k in (middle + j, quarter + j)] + list(range(middle + quarter, n_pairs)))
+        if s in DISPATCH_TICKS:
+            dispatch_later(DISPATCH_TICKS.index(s))
         if s == 0:
             pooled_in, halo = mix_local()
         if s == 2:

time: 90.2 us -> 88.7 us (0.983)
  the two profiles are of different devices: /device:TPU:2 before, /device:TPU:1 now
where the time goes in v4:
time: 88.7 us; the launch traced here: 87.1 us
  Pallas kernels  85 us (96%)
  local copies, waits for them, and re-layouts  1.4 us (2%)
    pallas_call x1, Pallas kernels, on_device(): pl.pallas_call(functools.partial(kernel, n_pairs), out_shape=jax.ShapeDty...  85 us

profile of v4, /device:TPU:1, one launch (start us, length us, event | category | flops | bytes accessed | tf_op | source)
XLA Modules:
  0.0 87.1 jit_solution(4281144032831608336)
XLA Ops:
  0.6 85.0 %shard_map.167 = bf16[2,128,128]{2,1,0:T(8,128)(2,1)} custom-call(bf16[128,2048]{1,0:T(8,128)(2,1)} %xe_hbm.1, bf16[128,2048]{1,0:T(8,128)(2,1)} %xm_hbm.1, f32[1,2048]{1,0:T(1,128)} %bitcast.14, f32[1,2048]{1,0:T(1,128)} %bitcast.15, bf16[64,2048]{1,0:T(8,128)(2,1)} %bitcast.12, f32[1,64]{1,0:T(1,128)} %bitcast.18, f32[1,64]{1,0:T(1,128)} %bitcast.19, ...), custom_call_target="tpu_custom_call" | custom-call | tf_op jit(solution)/shard_map/pallas_call | solution.py:500
  85.7 1.4 %slice_bitcast_fusion = (bf16[128,128]{1,0:T(8,128)(2,1)}, bf16[128,128]{1,0:T(8,128)(2,1)}) fusion(bf16[2,128,128]{2,1,0:T(8,128)(2,1)} %shard_map.167), kind=kLoop, calls=%fused_computation | loop fusion | bytes 131072 | tf_op jit(solution)/shard_map/squeeze | solution.py:566

commit v5 on v4

--- a/solution.py
+++ b/solution.py
@@ -164,7 +164,7 @@
         return send_sems.at[group // quarter if group < n_pairs else 4 + group - n_pairs]
 
     def recv_of(group, stage):
-        return recv_sems.at[group, stage] if group < n_pairs else rows_sems.at[group - n_pairs, stage]
+        return recv_sems.at[group % middle, stage] if group < n_pairs else rows_sems.at[group - n_pairs, stage]
 
     def launch(group, stage, src, dst, where):
         pltpu.make_async_remote_copy(
@@ -453,6 +453,8 @@
         if p := summed(s - LAGS["close"]):
             p.sum_finish(1)
             p.send_back()
+        if s == n_pairs - 1 + LAGS["second_relay"]:
+            result = plain_outputs()
         if p := summed(s - LAGS["second_relay"]):
             p.sum_relay(1)
         if p := summed(s - LAGS["second"]):
@@ -464,8 +466,6 @@
             p.gather_finish(1)
             p.compute()
             p.sum_start(0)
-        if s == n_pairs - 1 + LAGS["close"]:
-            result = plain_outputs()
 
     over = (((0,), (0,)), ((), ()))
     arrived = back.at[pl.ds(cap, rows_all - cap)]
@@ -533,7 +533,7 @@
             pltpu.VMEM((n_tp - 1, 8, LANES), F32),
             dma((11,)),
             dma((6,)),
-            dma((n_pairs, 8)),
+            dma((n_pairs // 2, 8)),
             dma((2, 4)),
             dma,
             dma((n_pairs,)),

time: 88.7 us -> 88.2 us (level)
  no operation moved by 1% of the time
where the time goes in v5:
time: 88.2 us; the launch traced here: 86.5 us
  Pallas kernels  84.5 us (96%)
  local copies, waits for them, and re-layouts  1.4 us (2%)
    pallas_call x1, Pallas kernels, on_device(): pl.pallas_call(functools.partial(kernel, n_pairs), out_shape=jax.ShapeDty...  84.5 us

profile of v5, /device:TPU:1, one launch (start us, length us, event | category | flops | bytes accessed | tf_op | source)
XLA Modules:
  0.0 86.5 jit_solution(16870480908822179539)
XLA Ops:
  0.6 84.5 %shard_map.167 = bf16[2,128,128]{2,1,0:T(8,128)(2,1)} custom-call(bf16[128,2048]{1,0:T(8,128)(2,1)} %xe_hbm.1, bf16[128,2048]{1,0:T(8,128)(2,1)} %xm_hbm.1, f32[1,2048]{1,0:T(1,128)} %bitcast.14, f32[1,2048]{1,0:T(1,128)} %bitcast.15, bf16[64,2048]{1,0:T(8,128)(2,1)} %bitcast.12, f32[1,64]{1,0:T(1,128)} %bitcast.18, f32[1,64]{1,0:T(1,128)} %bitcast.19, ...), custom_call_target="tpu_custom_call" | custom-call | tf_op jit(solution)/shard_map/pallas_call | solution.py:500
  85.1 1.4 %slice_bitcast_fusion = (bf16[128,128]{1,0:T(8,128)(2,1)}, bf16[128,128]{1,0:T(8,128)(2,1)}) fusion(bf16[2,128,128]{2,1,0:T(8,128)(2,1)} %shard_map.167), kind=kLoop, calls=%fused_computation | loop fusion | bytes 131072 | tf_op jit(solution)/shard_map/squeeze | solution.py:566
